TPU v7x, 32 devices: a whole 2x2x4 slice. The times are simulated.
32 devices in a mesh: sp: 8 (over z, y), tp: 4 (over x, core).
Axes of the slice: x: 2, y: 2, z: 4, core: 2. Of those that a mesh axis runs over, the one named last changes fastest.
Arguments:
- gate_branch: bfloat16 [6144, 1024], P('sp', 'tp'), may hold values from -6 to 6
- recur_input: bfloat16 [6144, 1024], P('sp', 'tp'), may hold values from -6 to 6
- doc_ids: int32 [6144], P('sp'), may hold values from 0 to 3, never falling along the last dimension, each value on 1 to 4608 neighbouring positions
- conv_taps: bfloat16 [4, 1024], P(None, 'tp'), may hold values from -3 to 3
- gate_map: bfloat16 [16, 64, 64], P('tp'), may hold values from -0.75 to 0.75
- input_map: bfloat16 [16, 64, 64], P('tp'), may hold values from -0.75 to 0.75
- decay_level: float32 [1024], P('tp'), may hold values from 4.8 to 12.3
- decay_extra: float32 [6144, 1024], P('sp', 'tp'), may hold values from -2.1 to -1.9e-05
- out_weight: bfloat16 [1024, 2048], P(None, 'tp'), may hold values from -0.7875 to 0.7875
- residual: bfloat16 [6144, 2048], P('sp', 'tp'), may hold values from -44 to 44
- mix_gain: float32 [2048], P('tp'), may hold values from 0.1 to 1.9
- pre_gain: float32 [2048], P('tp'), may hold values from 0.1 to 1.9
- ffn_gain: float32 [2048], P('tp'), may hold values from 0.1 to 1.9
- gate_weight: bfloat16 [2048, 5632], P('sp', 'tp'), may hold values from -0.125 to 0.125
- up_weight: bfloat16 [2048, 5632], P('sp', 'tp'), may hold values from -0.125 to 0.125
- down_weight: bfloat16 [5632, 2048], P('tp', 'sp'), may hold values from -0.33579113 to 0.33579113
Outputs:
- layer_out: bfloat16 [6144, 2048], P('sp', 'tp')
Inputs may be any that keep to these rules, and one draw needn't show every extreme that they name: `doc_ids`: document numbers start at 0 and never fall along the sequence; a document has 1 to 4608 positions, and one has exactly that many.
All inputs are finite; a program needn't handle non-finite values.
Results may differ from a plain program's by a relative error of at most 0.013.
Values may be sent and summed in bfloat16 or wider, within the bound.
A program may use at most 64 MiB of HBM per device.

v0:
```python
import functools
import math

import jax
import jax.numpy as jnp
from jax import lax
from jax.experimental import pallas as pl
from jax.experimental.pallas import tpu as pltpu
from jax.sharding import PartitionSpec as P

EPS = 1e-06
GATE_POWER = 8.0
F32 = jnp.float32
BF16 = jnp.bfloat16
MESH = pl.DeviceIdType.MESH


def grid_of(n):
    ny = 1
    for c in range(1, n + 1):
        if n % c == 0 and c * c <= n:
            ny = c
    return n // ny, ny


def ring_pos(s, nz, ny):
    z, y = lax.div(s, ny), lax.rem(s, ny)
    off = lax.div(y + ny - 1, ny)
    r = nz - 1 - z
    odd = lax.rem(r, 2)
    within = (1 - odd) * (y - 1) + odd * (ny - 1 - y)
    return (1 - off) * z + off * (nz + r * (ny - 1) + within)


def ring_dev(p, nz, ny):
    off = lax.div(lax.div(p, nz) + ny - 1, ny)
    q = off * (p - nz)
    r = lax.div(q, ny - 1)
    w = lax.rem(q, ny - 1)
    odd = lax.rem(r, 2)
    y = (1 - odd) * (1 + w) + odd * (ny - 1 - w)
    return (1 - off) * (p * ny) + off * ((nz - 1 - r) * ny + y)


def one_minus_exp(u):
    series = 1.0 + u * (1 / 8)
    for k in (7, 6, 5, 4, 3, 2):
        series = 1.0 + u * (1.0 / k) * series
    return jnp.where(u > -0.35, -u * series, 1.0 - jnp.exp(u))


def kernel(
    cfg,
    gate_branch, recur, ids, taps, gmap, imap, rate, extra, out_w, residual,
    mix_gain, pre_gain, ffn_gain, gate_w, up_w, down_w,
    out,
    gate_all, up_all, down_all, xpad, idpad, halo, ihalo, bd, fac, drv, ends, bfull,
    mixed, normed, hidden, partial, shared, recvd, own, ssq,
    wsend, wrecv, lsem, hsend, hrecv, esend, erecv, bsend, brecv, nsend, nrecv, qsend, qrecv, psend, precv, msem,
):
    n, ntp, nz, ny, width = cfg
    s, t = lax.axis_index("sp"), lax.axis_index("tp")
    tok, loc = recur.shape
    dloc = residual.shape[1]
    krows = gate_w.shape[0]
    ncol = down_w.shape[1]
    ff = gate_w.shape[1]
    CH = math.gcd(tok, 64)
    BR = math.gcd(tok, 128)
    pos = ring_pos(s, nz, ny)

    barrier = pltpu.get_barrier_semaphore()
    for j in range(1, n):
        pl.semaphore_signal(barrier, inc=1, device_id=(lax.rem(s + j, n), t), device_id_type=MESH)
    for j in range(1, ntp):
        pl.semaphore_signal(barrier, inc=1, device_id=(s, lax.rem(t + j, ntp)), device_id_type=MESH)
    pl.semaphore_wait(barrier, n - 1 + ntp - 1)

    shard = (gate_w, up_w, down_w)
    whole = (gate_all, up_all, down_all)
    nxt = [ring_dev(lax.rem(pos + 1, n), nz, ny), ring_dev(lax.rem(pos + n - 1, n), nz, ny)]
    origin = [[s] + [ring_dev(lax.rem(pos + (n - k if d == 0 else k), n), nz, ny) for k in range(1, n)] for d in range(2)]

    def half(a, o, d, local=False):
        if a < 2:
            h = krows // 2
            if local:
                return shard[a].at[pl.ds(d * h, h)]
            return whole[a].at[pl.ds(pl.multiple_of(o * krows + d * h, h), h)]
        h = ff // 2
        if local:
            return shard[a].at[pl.ds(d * h, h)]
        return whole[a].at[o, pl.ds(d * h, h)]

    def ring(a, d, k):
        o = origin[d][k]
        return pltpu.make_async_remote_copy(
            src_ref=half(a, o, d, k == 0), dst_ref=half(a, o, d),
            send_sem=wsend.at[a, d, k], recv_sem=wrecv.at[a, d, k],
            device_id=(nxt[d], t), device_id_type=MESH)

    def arrived(a, d, k):
        o = origin[d][k + 1]
        pltpu.make_async_remote_copy(
            src_ref=half(a, o, d), dst_ref=half(a, o, d),
            send_sem=wsend.at[a, d, k], recv_sem=wrecv.at[a, d, k],
            device_id=(nxt[d], t), device_id_type=MESH).wait_recv()

    def serve(arrays, k):
        for a in arrays:
            for d in range(2):
                arrived(a, d, k)
                if k < n - 2:
                    ring(a, d, k + 1).start()

    for a in range(3):
        for d in range(2):
            ring(a, d, 0).start()

    def halo_copy(i):
        src, dst = ((recur.at[pl.ds(tok - 16, 16)], halo), (ids.at[pl.ds(tok - 8, 8)], ihalo))[i]
        return pltpu.make_async_remote_copy(
            src_ref=src, dst_ref=dst, send_sem=hsend.at[i], recv_sem=hrecv.at[i],
            device_id=(lax.rem(s + 1, n), t), device_id_type=MESH)

    for i in range(2):
        halo_copy(i).start()

    def local_copy(a):
        if a < 2:
            dst = whole[a].at[pl.ds(pl.multiple_of(s * krows, krows), krows)]
        else:
            dst = whole[a].at[s]
        return pltpu.make_async_copy(shard[a], dst, lsem.at[a])

    for a in range(3):
        local_copy(a).start()

    head = gmap.shape[1]
    spread = (lax.rem(lax.broadcasted_iota(jnp.int32, (head, loc), 1), head)
              == lax.broadcasted_iota(jnp.int32, (head, loc), 0)).astype(BF16)
    diag = (lax.div(lax.broadcasted_iota(jnp.int32, (loc, loc), 0), head)
            == lax.div(lax.broadcasted_iota(jnp.int32, (loc, loc), 1), head))
    for i, m in enumerate((gmap, imap)):
        tiled = jnp.dot(m[...], spread, preferred_element_type=F32)
        bd[i] = jnp.where(diag, tiled, 0.0).astype(BF16)

    for i in range(2):
        halo_copy(i).wait()
    first = s == 0
    xpad[pl.ds(0, 8)] = halo[...].astype(F32)[8:16]
    idpad[pl.ds(0, 8)] = jnp.where(first, -1, ihalo[...])

    def fill(i, _):
        r = pl.multiple_of(i * CH, CH)
        xpad[pl.ds(pl.multiple_of(r + 8, 8), CH)] = recur[pl.ds(r, CH)].astype(F32)
        idpad[pl.ds(pl.multiple_of(r + 8, 8), CH)] = ids[pl.ds(r, CH)]
        return 0

    lax.fori_loop(0, tok // CH, fill, 0)
    reps = loc // 128
    ntaps = taps.shape[0]

    def front(i, _):
        r = pl.multiple_of(i * CH, CH)
        xw = xpad[pl.ds(r, CH + 8)]
        iw = idpad[pl.ds(r, CH + 8)]
        mine = iw[8:]
        tw = taps[...]
        conv = xw[8:] * tw[0:1]
        cont = None
        for k in range(1, ntaps):
            same1 = (pltpu.roll(iw, k, axis=0)[8:] == mine).astype(F32)
            same = jnp.concatenate([same1] * reps, axis=1)
            if k == 1:
                cont = same
            conv = conv + same * pltpu.roll(xw, k, axis=0)[8:] * tw[k:k + 1]
        cb = conv.astype(BF16)
        rg = jax.nn.sigmoid(jnp.dot(cb, bd[0], preferred_element_type=F32))
        ig = jax.nn.sigmoid(jnp.dot(cb, bd[1], preferred_element_type=F32))
        ld = rate[...] * rg + extra[pl.ds(r, CH)]
        fac[pl.ds(r, CH)] = jnp.exp(ld) * cont
        drv[pl.ds(r, CH)] = jnp.sqrt(one_minus_exp(2.0 * ld)) * ig * cb.astype(F32)
        return 0

    lax.fori_loop(0, tok // CH, front, 0)

    rows8 = lax.broadcasted_iota(jnp.int32, (8, loc), 0)

    def scan(i, carry):
        pc, hc = carry
        r = pl.multiple_of(i * 8, 8)
        a, b = fac[pl.ds(r, 8)], drv[pl.ds(r, 8)]
        for sh in (1, 2, 4):
            keep = rows8 >= sh
            b = b + a * jnp.where(keep, pltpu.roll(b, sh, axis=0), 0.0)
            a = a * jnp.where(keep, pltpu.roll(a, sh, axis=0), 1.0)
        h = b + a * hc
        p = a * pc
        fac[pl.ds(r, 8)] = p
        drv[pl.ds(r, 8)] = h
        return (jnp.broadcast_to(p[7:8], (8, loc)), jnp.broadcast_to(h[7:8], (8, loc)))

    pend, hend = lax.fori_loop(0, tok // 8, scan, (jnp.ones((8, loc), F32), jnp.zeros((8, loc), F32)))
    ends[s] = jnp.concatenate([pend, hend], axis=0)

    def end_copy(j):
        return pltpu.make_async_remote_copy(
            src_ref=ends.at[s], dst_ref=ends.at[s], send_sem=esend.at[j - 1], recv_sem=erecv.at[j - 1],
            device_id=(lax.rem(s + j, n), t), device_id_type=MESH)

    def end_arrived(j):
        o = lax.rem(s + n - j, n)
        pltpu.make_async_remote_copy(
            src_ref=ends.at[o], dst_ref=ends.at[o], send_sem=esend.at[j - 1], recv_sem=erecv.at[j - 1],
            device_id=(lax.rem(s + j, n), t), device_id_type=MESH).wait_recv()

    for j in range(1, n):
        end_copy(j).start()
    serve((0, 1), 0)
    for j in range(1, n):
        end_arrived(j)
    carry = jnp.zeros((8, loc), F32)
    for o in range(n - 1):
        e = ends[o]
        carry = jnp.where(o < s, e[:8] * carry + e[8:], carry)
    cin = carry[0:1]

    def branch(i, _):
        r = pl.multiple_of(i * CH, CH)
        st = drv[pl.ds(r, CH)] + fac[pl.ds(r, CH)] * cin
        bfull[t, pl.ds(r, CH)] = (st * jax.nn.gelu(gate_branch[pl.ds(r, CH)].astype(F32))).astype(BF16)
        return 0

    lax.fori_loop(0, tok // CH, branch, 0)

    def tp_push(view, send, recv, j, start):
        o = t if start else lax.rem(t + ntp - j, ntp)
        return pltpu.make_async_remote_copy(
            src_ref=view(o), dst_ref=view(o), send_sem=send.at[j - 1], recv_sem=recv.at[j - 1],
            device_id=(s, lax.rem(t + j, ntp)), device_id_type=MESH)

    def bview(o):
        return bfull.at[o]

    chips = ntp // 2
    core = lax.rem(t, 2)
    mate = t + 1 - 2 * core

    def far(view, send, recv, c, start):
        o = t if start else lax.rem(t + ntp - 2 * c, ntp)
        return pltpu.make_async_remote_copy(
            src_ref=view(o), dst_ref=view(o), send_sem=send.at[c - 1], recv_sem=recv.at[c - 1],
            device_id=(s, lax.rem(t + 2 * c, ntp)), device_id_type=MESH)

    def near(view, send, recv, c, start):
        base = t if start else mate
        o = lax.rem(base + ntp - 2 * c, ntp)
        return pltpu.make_async_remote_copy(
            src_ref=view(o), dst_ref=view(o), send_sem=send.at[chips - 1 + c], recv_sem=recv.at[chips - 1 + c],
            device_id=(s, mate), device_id_type=MESH)

    def gather_start(view, send, recv):
        for c in range(1, chips):
            far(view, send, recv, c, True).start()
        near(view, send, recv, 0, True).start()

    def gather_share(view, send, recv):
        for c in range(1, chips):
            far(view, send, recv, c, False).wait_recv()
            near(view, send, recv, c, True).start()

    def gather_wait(view, send, recv):
        for c in range(chips):
            near(view, send, recv, c, False).wait_recv()

    def gather_sent(view, send, recv):
        for c in range(1, chips):
            far(view, send, recv, c, True).wait_send()
        for c in range(chips):
            near(view, send, recv, c, True).wait_send()

    gather_start(bview, bsend, brecv)
    serve((0, 1), 1)
    gather_share(bview, bsend, brecv)
    gather_wait(bview, bsend, brecv)

    def row_total(q, values):
        def write(i, _):
            r = pl.multiple_of(i * BR, BR)
            v = values(r)
            c = jnp.sum(v * v, axis=1, keepdims=True)
            ssq[q, t, :, pl.ds(r, BR)] = jnp.transpose(jnp.broadcast_to(c, (BR, 128)))[:8]
            return 0

        lax.fori_loop(0, tok // BR, write, 0)
        for j in range(1, ntp):
            tp_push(lambda o: ssq.at[q, o], qsend.at[q], qrecv.at[q], j, True).start()

    def wait_total(q):
        for j in range(1, ntp):
            tp_push(lambda o: ssq.at[q, o], qsend.at[q], qrecv.at[q], j, False).wait_recv()

    def inverse_rms(q, r):
        row = ssq[q, 0, 0:1, pl.ds(r, BR)]
        for o in range(1, ntp):
            row = row + ssq[q, o, 0:1, pl.ds(r, BR)]
        inv = lax.rsqrt(row / width + EPS)
        return jnp.transpose(jnp.broadcast_to(inv, (128, BR)))[:, 0:1]

    def project(i, _):
        r = pl.multiple_of(i * BR, BR)
        total = jnp.zeros((BR, dloc), F32)
        for o in range(ntp):
            total += jnp.dot(bfull[o, pl.ds(r, BR)], out_w[pl.ds(o * loc, loc)], preferred_element_type=F32)
        mixed[pl.ds(r, BR)] = total.astype(BF16)
        return 0

    lax.fori_loop(0, tok // BR, project, 0)
    row_total(0, lambda r: mixed[pl.ds(r, BR)].astype(F32))
    wait_total(0)

    def stream(i, _):
        r = pl.multiple_of(i * BR, BR)
        m = mixed[pl.ds(r, BR)].astype(F32)
        mixed[pl.ds(r, BR)] = (residual[pl.ds(r, BR)].astype(F32) + m * inverse_rms(0, r) * mix_gain[...]).astype(BF16)
        return 0

    lax.fori_loop(0, tok // BR, stream, 0)
    row_total(1, lambda r: mixed[pl.ds(r, BR)].astype(F32))
    serve((0, 1), 2)
    wait_total(1)

    def norm(i, _):
        r = pl.multiple_of(i * BR, BR)
        m = mixed[pl.ds(r, BR)].astype(F32)
        normed[pl.ds(r, BR), pl.ds(pl.multiple_of(t * dloc, dloc), dloc)] = (m * inverse_rms(1, r) * pre_gain[...]).astype(BF16)
        return 0

    lax.fori_loop(0, tok // BR, norm, 0)

    def nview(o):
        return normed.at[:, pl.ds(pl.multiple_of(o * dloc, dloc), dloc)]

    gather_start(nview, nsend, nrecv)
    serve((0, 1), 3)
    gather_share(nview, nsend, nrecv)
    for k in range(4, n - 2):
        serve((0, 1), k)
    serve((2,), 0)
    serve((0, 1), n - 2)
    gather_wait(nview, nsend, nrecv)
    for a in range(3):
        local_copy(a).wait()

    def ffn_tile(c, size):
        cols = pl.ds(c, size)
        g = jnp.dot(normed[...], gate_all[:, cols], preferred_element_type=F32)
        u = jnp.dot(normed[...], up_all[:, cols], preferred_element_type=F32)
        hidden[:, cols] = (jax.nn.silu(g) * u).astype(BF16)

    TN = 256
    tiles = ff // TN

    def ffn_step(j, _):
        ffn_tile(pl.multiple_of(j * TN, TN), TN)
        return 0

    cut = (tiles + 1) // 2
    lax.fori_loop(0, cut, ffn_step, 0)
    serve((2,), 1)
    lax.fori_loop(cut, tiles, ffn_step, 0)
    if ff % TN:
        ffn_tile(tiles * TN, ff % TN)

    per = dloc // ncol

    def place(o):
        c = lax.div(o, per)
        w = lax.rem(o, per)
        gap = lax.rem(lax.div(c, 2) - lax.div(t, 2) + chips, chips)
        return lax.rem(c, 2), w, c, gap

    def mate_copy(i):
        return pltpu.make_async_remote_copy(
            src_ref=partial.at[i], dst_ref=shared.at[i], send_sem=psend.at[i], recv_sem=msem.at[i],
            device_id=(s, mate), device_id_type=MESH)

    def far_copy(i, w, c, gap):
        g = lax.rem(gap + chips - 1, chips)
        return pltpu.make_async_remote_copy(
            src_ref=partial.at[i], dst_ref=recvd.at[g, w], send_sem=psend.at[i], recv_sem=precv.at[g, w],
            device_id=(s, c), device_id_type=MESH)

    sent = []

    def down(*blocks):
        for o in blocks:
            i = len(sent)
            sent.append(o)
            partial[i] = jnp.dot(hidden[...], down_all[o], preferred_element_type=F32).astype(BF16)
            par, w, c, gap = place(o)

            @pl.when(par != core)
            def _():
                mate_copy(i).start()

    def join(i):
        par, w, c, gap = place(sent[i])

        @pl.when(par == core)
        def _():
            mate_copy(i).wait_recv()

            def add(b, _):
                r = pl.multiple_of(b * BR, BR)
                total = partial[i, pl.ds(r, BR)].astype(F32) + shared[i, pl.ds(r, BR)].astype(F32)
                partial[i, pl.ds(r, BR)] = total.astype(BF16)
                return 0

            lax.fori_loop(0, tok // BR, add, 0)

            @pl.when(gap == 0)
            def _():
                own[w] = partial[i]

            @pl.when(gap != 0)
            def _():
                far_copy(i, w, c, gap).start()

    down(s)
    joined = 0
    for k in range(2, n - 1):
        serve((2,), k)
        have = k + 1
        if 2 * have >= n:
            if 2 * have == n:
                down(origin[0][have])
            else:
                down(origin[0][have], origin[0][n - have])
        if k == n - 2:
            upto = len(sent)
        else:
            upto = len(sent) - (1 if 2 * have == n else 2) if 2 * have >= n else len(sent)
        while joined < upto:
            join(joined)
            joined += 1

    for i, o in enumerate(sent):
        par, w, c, gap = place(o)

        @pl.when(par != core)
        def _():
            mate_copy(i).wait_send()

        @pl.when(par == core)
        def _():
            @pl.when(gap != 0)
            def _():
                far_copy(i, w, c, gap).wait_send()

    for g in range(1, chips):
        for w in range(per):
            pltpu.make_async_remote_copy(
                src_ref=partial.at[0], dst_ref=recvd.at[g - 1, w],
                send_sem=psend.at[0], recv_sem=precv.at[g - 1, w],
                device_id=(s, mate), device_id_type=MESH).wait_recv()

    def gather_sum(i, _):
        r = pl.multiple_of(i * BR, BR)
        for w in range(per):
            total = own[w, pl.ds(r, BR)].astype(F32)
            for j in range(chips - 1):
                total = total + recvd[j, w, pl.ds(r, BR)].astype(F32)
            out[pl.ds(r, BR), pl.ds(w * ncol, ncol)] = total.astype(BF16)
        return 0

    lax.fori_loop(0, tok // BR, gather_sum, 0)
    row_total(2, lambda r: out[pl.ds(r, BR)].astype(F32))
    wait_total(2)

    def finish(i, _):
        r = pl.multiple_of(i * BR, BR)
        f = out[pl.ds(r, BR)].astype(F32)
        out[pl.ds(r, BR)] = (mixed[pl.ds(r, BR)].astype(F32) + f * inverse_rms(2, r) * ffn_gain[...]).astype(BF16)
        return 0

    lax.fori_loop(0, tok // BR, finish, 0)

    for a in range(3):
        for d in range(2):
            for k in range(n - 1):
                ring(a, d, k).wait_send()
    for j in range(1, n):
        end_copy(j).wait_send()
    gather_sent(bview, bsend, brecv)
    gather_sent(nview, nsend, nrecv)
    for j in range(1, ntp):
        for q in range(3):
            tp_push(lambda o: ssq.at[q, o], qsend.at[q], qrecv.at[q], j, True).wait_send()


def body(n, ntp, gate_branch, recur_input, doc_ids, conv_taps, gate_map, input_map, decay_level, decay_extra,
         out_weight, residual, mix_gain, pre_gain, ffn_gain, gate_weight, up_weight, down_weight):
    tok, loc = recur_input.shape
    dloc = residual.shape[1]
    krows, ff = gate_weight.shape
    ncol = down_weight.shape[1]
    heads, head, _ = gate_map.shape
    nz, ny = grid_of(n)
    ids = jnp.broadcast_to(doc_ids[:, None], (tok, 128))
    rate = (GATE_POWER * -jax.nn.softplus(-decay_level))[None, :]
    args = (gate_branch, recur_input, ids, conv_taps.astype(F32), gate_map.reshape(heads * head, head),
            input_map.reshape(heads * head, head), rate, decay_extra, out_weight, residual,
            mix_gain[None, :], pre_gain[None, :], ffn_gain[None, :], gate_weight, up_weight, down_weight)
    vm = pl.BlockSpec(memory_space=pltpu.VMEM)
    hbm = pl.BlockSpec(memory_space=pl.ANY)
    V, S = pltpu.VMEM, pltpu.SemaphoreType.DMA
    per = dloc // ncol
    chips = ntp // 2
    return pl.pallas_call(
        functools.partial(kernel, (n, ntp, nz, ny, dloc * ntp)),
        out_shape=jax.ShapeDtypeStruct((tok, dloc), BF16),
        in_specs=[vm] * 13 + [hbm] * 3,
        out_specs=vm,
        scratch_shapes=[
            V((n * krows, ff), BF16), V((n * krows, ff), BF16), V((n, ff, ncol), BF16),
            V((tok + 8, loc), F32), V((tok + 8, 128), jnp.int32), V((16, loc), BF16), V((8, 128), jnp.int32),
            V((2, loc, loc), BF16), V((tok, loc), F32), V((tok, loc), F32), V((n, 16, loc), F32),
            V((ntp, tok, loc), BF16), V((tok, dloc), BF16), V((tok, dloc * ntp), BF16), V((tok, ff), BF16),
            V((n, tok, ncol), BF16), V((n, tok, ncol), BF16), V((chips - 1, per, tok, ncol), BF16), V((per, tok, ncol), BF16),
            V((3, ntp, 8, tok), F32),
            S((3, 2, n - 1)), S((3, 2, n - 1)), S((3,)), S((2,)), S((2,)), S((n - 1,)), S((n - 1,)),
            S((ntp - 1,)), S((ntp - 1,)), S((ntp - 1,)), S((ntp - 1,)), S((3, ntp - 1)), S((3, ntp - 1)),
            S((n,)), S((chips - 1, per)), S((n,)),
        ],
        compiler_params=pltpu.CompilerParams(
            collective_id=0, has_side_effects=True, vmem_limit_bytes=62 * 1024 * 1024),
    )(*args)


def solution(mesh):
    in_specs = (
        P("sp", "tp"), P("sp", "tp"), P("sp"), P(None, "tp"), P("tp", None, None), P("tp", None, None),
        P("tp"), P("sp", "tp"), P(None, "tp"), P("sp", "tp"), P("tp"), P("tp"), P("tp"),
        P("sp", "tp"), P("sp", "tp"), P("tp", "sp"),
    )
    fn = functools.partial(body, mesh.shape["sp"], mesh.shape["tp"])
    return jax.shard_map(fn, mesh=mesh, in_specs=in_specs, out_specs=P("sp", "tp"), check_vma=False)
```

profile of v0, /device:TPU:0, one launch (start us, length us, event | category | flops | bytes accessed | tf_op | source)
XLA Modules:
  0.0 207.2 jit_solution(2294683773908550617)
XLA Ops:
  0.0 0.0 copy-start.2
  0.0 0.7 copy-done.2
  0.7 0.0 copy-start.1
  0.7 0.6 fusion.1
  1.2 0.0 copy-start
  1.2 0.1 copy-done.1
  1.4 0.6 convert_element_type.3.taps
  1.9 0.0 copy-done
  2.0 0.9 broadcast_in_dim.18.ids
  2.9 202.3 %shard_map.154 = bf16[768,512]{1,0:T(8,128)(2,1)} custom-call(bf16[768,256]{1,0:T(8,128)(2,1)} %gate_branch.1, bf16[768,256]{1,0:T(8,128)(2,1)} %recur.1, s32[768,128]{1,0:T(8,128)} %broadcast_in_dim.18.ids, f32[4,256]{1,0:T(4,128)} %convert_element_type.3.taps, bf16[256,64]{1,0:T(8,128)(2,1)} %bitcast.6, bf16[256,64]{1,0:T(8,128)(2,1)} %bitcast.7, ...), custom_call_target="tpu_custom_call" | custom-call | tf_op jit(solution)/shard_map/pallas_call | solution.py:521
  205.1 2.1 copy.18
Async XLA Ops:
  0.0 0.7 copy-start.2
  0.7 0.7 copy-start.1
  1.2 0.7 copy-start
where the time goes:
time: 211 us; the launch traced here: 207 us
  Pallas kernels  202 us (96%)
  local copies, waits for them, and re-layouts  3.77 us (2%)
    pallas_call x1, Pallas kernels, body(): pl.pallas_call(functools.partial(kernel, (n, ntp, nz, ny, dloc * ntp)), o...  202 us

commit v1 on v0

--- a/solution.py
+++ b/solution.py
@@ -500,6 +500,516 @@
             tp_push(lambda o: ssq.at[q, o], qsend.at[q], qrecv.at[q], j, True).wait_send()
 
 
+def plane_kernel(
+    cfg,
+    gate_branch, recur, ids, taps, gmap, imap, rate, extra, out_w, residual,
+    mix_gain, pre_gain, ffn_gain, gate_w, up_w, down_w,
+    out,
+    gate_all, up_all, down_all, xpad, idpad, halo, ihalo, bd, fac, drv, ends, bfull,
+    mixed, nloc, normed, hidden, partial, recvd, ssq,
+    lsem, ssend, srecv, zsend, zrecv, msend, mrecv,
+    hsend, hrecv, esend, erecv, bsend, brecv, nsend, nrecv, qsend, qrecv, psend, precv,
+):
+    n, ntp, nz, ny, width = cfg
+    s, t = lax.axis_index("sp"), lax.axis_index("tp")
+    tok, loc = recur.shape
+    dloc = residual.shape[1]
+    krows = gate_w.shape[0]
+    ncol = down_w.shape[1]
+    ff = gate_w.shape[1]
+    CH = math.gcd(tok, 64)
+    BR = math.gcd(tok, 128)
+    chips = ntp // 2
+    z, y = lax.div(s, ny), lax.rem(s, ny)
+    x, core = lax.div(t, 2), lax.rem(t, 2)
+    mate = t + 1 - 2 * core
+    per = dloc // ncol
+
+    barrier = pltpu.get_barrier_semaphore()
+    peers = [(z * ny + lax.rem(y + dy, ny), lax.rem(t + dt, ntp)) for dy in range(ny) for dt in range(ntp)][1:]
+    peers += [(lax.rem(z + dz, nz) * ny + lax.rem(y + dy, ny), t) for dz in range(1, nz) for dy in range(ny)]
+    for p in peers:
+        pl.semaphore_signal(barrier, inc=1, device_id=p, device_id_type=MESH)
+    pl.semaphore_wait(barrier, len(peers))
+
+    shard = (gate_w, up_w, down_w)
+    whole = (gate_all, up_all, down_all)
+    low = (2 * z < nz).astype(jnp.int32)
+    near_first = []
+    for k in range(1, nz):
+        near_first += [z + (2 * low - 1) * k, z - (2 * low - 1) * k]
+    origin = [z]
+    seen = 0
+    ranks = []
+    for q in near_first:
+        ok = jnp.logical_and(q >= 0, q < nz).astype(jnp.int32)
+        seen = seen + ok
+        ranks.append((q, ok, seen))
+    for j in range(1, nz):
+        origin.append(sum(jnp.where(jnp.logical_and(ok == 1, r == j), q, 0) for q, ok, r in ranks))
+
+    def block(a, o, b):
+        i = o * ny + b
+        if a < 2:
+            return whole[a].at[pl.ds(pl.multiple_of(i * krows, krows), krows)]
+        return whole[a].at[i]
+
+    def seed_local(a):
+        return pltpu.make_async_copy(shard[a], block(a, z, y), lsem.at[a])
+
+    def seed_swap(a):
+        return pltpu.make_async_remote_copy(
+            src_ref=shard[a], dst_ref=block(a, z, y), send_sem=ssend.at[a], recv_sem=srecv.at[a],
+            device_id=(z * ny + 1 - y, mate), device_id_type=MESH)
+
+    def z_copy(a, o, up):
+        b = block(a, o, core)
+        return pltpu.make_async_remote_copy(
+            src_ref=b, dst_ref=b, send_sem=zsend.at[up, a, o], recv_sem=zrecv.at[a, o],
+            device_id=((z + 2 * up - 1) * ny + y, t), device_id_type=MESH)
+
+    def mate_copy(a, o, theirs=False):
+        b = block(a, o, 1 - core if theirs else core)
+        return pltpu.make_async_remote_copy(
+            src_ref=b, dst_ref=b, send_sem=msend.at[a, o], recv_sem=mrecv.at[a, o],
+            device_id=(s, mate), device_id_type=MESH)
+
+    def fan_down(a, o, act):
+        @pl.when(jnp.logical_and(o >= z, z > 0))
+        def _():
+            act(z_copy(a, o, 0))
+
+    def fan_up(a, o, act):
+        @pl.when(jnp.logical_and(o <= z, z < nz - 1))
+        def _():
+            act(z_copy(a, o, 1))
+
+    def fan(a, o, act):
+        fan_down(a, o, act)
+        fan_up(a, o, act)
+        act(mate_copy(a, o))
+
+    def start(c):
+        c.start()
+
+    def push_seed(a):
+        @pl.when(y == core)
+        def _():
+            seed_local(a).wait()
+
+        @pl.when(y != core)
+        def _():
+            pltpu.make_async_remote_copy(
+                src_ref=block(a, z, core), dst_ref=block(a, z, core), send_sem=ssend.at[a], recv_sem=srecv.at[a],
+                device_id=(z * ny + 1 - y, mate), device_id_type=MESH).wait_recv()
+
+        fan(a, z, start)
+
+    def relay(a, j):
+        o = origin[j]
+        z_copy(a, o, 0).wait_recv()
+        fan(a, o, start)
+
+    for a in range(3):
+        @pl.when(y == core)
+        def _():
+            seed_local(a).start()
+
+        @pl.when(y != core)
+        def _():
+            seed_swap(a).start()
+
+    def halo_copy(i):
+        src, dst = ((recur.at[pl.ds(tok - 16, 16)], halo), (ids.at[pl.ds(tok - 8, 8)], ihalo))[i]
+        return pltpu.make_async_remote_copy(
+            src_ref=src, dst_ref=dst, send_sem=hsend.at[i], recv_sem=hrecv.at[i],
+            device_id=(lax.rem(s + 1, n), t), device_id_type=MESH)
+
+    for i in range(2):
+        halo_copy(i).start()
+
+    @pl.when(y == core)
+    def _():
+        push_seed(0)
+        push_seed(1)
+
+    head = gmap.shape[1]
+    spread = (lax.rem(lax.broadcasted_iota(jnp.int32, (head, loc), 1), head)
+              == lax.broadcasted_iota(jnp.int32, (head, loc), 0)).astype(BF16)
+    diag = (lax.div(lax.broadcasted_iota(jnp.int32, (loc, loc), 0), head)
+            == lax.div(lax.broadcasted_iota(jnp.int32, (loc, loc), 1), head))
+    for i, m in enumerate((gmap, imap)):
+        tiled = jnp.dot(m[...], spread, preferred_element_type=F32)
+        bd[i] = jnp.where(diag, tiled, 0.0).astype(BF16)
+
+    for i in range(2):
+        halo_copy(i).wait()
+    first = s == 0
+    xpad[pl.ds(0, 8)] = halo[...].astype(F32)[8:16]
+    idpad[pl.ds(0, 8)] = jnp.where(first, -1, ihalo[...])
+
+    def fill(i, _):
+        r = pl.multiple_of(i * CH, CH)
+        xpad[pl.ds(pl.multiple_of(r + 8, 8), CH)] = recur[pl.ds(r, CH)].astype(F32)
+        idpad[pl.ds(pl.multiple_of(r + 8, 8), CH)] = ids[pl.ds(r, CH)]
+        return 0
+
+    lax.fori_loop(0, tok // CH, fill, 0)
+
+    @pl.when(y != core)
+    def _():
+        push_seed(0)
+
+    reps = loc // 128
+    ntaps = taps.shape[0]
+
+    def front(i, _):
+        r = pl.multiple_of(i * CH, CH)
+        xw = xpad[pl.ds(r, CH + 8)]
+        iw = idpad[pl.ds(r, CH + 8)]
+        mine = iw[8:]
+        tw = taps[...]
+        conv = xw[8:] * tw[0:1]
+        cont = None
+        for k in range(1, ntaps):
+            same1 = (pltpu.roll(iw, k, axis=0)[8:] == mine).astype(F32)
+            same = jnp.concatenate([same1] * reps, axis=1)
+            if k == 1:
+                cont = same
+            conv = conv + same * pltpu.roll(xw, k, axis=0)[8:] * tw[k:k + 1]
+        cb = conv.astype(BF16)
+        rg = jax.nn.sigmoid(jnp.dot(cb, bd[0], preferred_element_type=F32))
+        ig = jax.nn.sigmoid(jnp.dot(cb, bd[1], preferred_element_type=F32))
+        ld = rate[...] * rg + extra[pl.ds(r, CH)]
+        fac[pl.ds(r, CH)] = jnp.exp(ld) * cont
+        drv[pl.ds(r, CH)] = jnp.sqrt(one_minus_exp(2.0 * ld)) * ig * cb.astype(F32)
+        return 0
+
+    lax.fori_loop(0, tok // CH, front, 0)
+
+    @pl.when(y != core)
+    def _():
+        push_seed(1)
+
+    rows8 = lax.broadcasted_iota(jnp.int32, (8, loc), 0)
+
+    def scan(i, carry):
+        pc, hc = carry
+        r = pl.multiple_of(i * 8, 8)
+        a, b = fac[pl.ds(r, 8)], drv[pl.ds(r, 8)]
+        for sh in (1, 2, 4):
+            keep = rows8 >= sh
+            b = b + a * jnp.where(keep, pltpu.roll(b, sh, axis=0), 0.0)
+            a = a * jnp.where(keep, pltpu.roll(a, sh, axis=0), 1.0)
+        h = b + a * hc
+        p = a * pc
+        fac[pl.ds(r, 8)] = p
+        drv[pl.ds(r, 8)] = h
+        return (jnp.broadcast_to(p[7:8], (8, loc)), jnp.broadcast_to(h[7:8], (8, loc)))
+
+    pend, hend = lax.fori_loop(0, tok // 8, scan, (jnp.ones((8, loc), F32), jnp.zeros((8, loc), F32)))
+    ends[s] = jnp.concatenate([pend, hend], axis=0)
+
+    def end_copy(j):
+        return pltpu.make_async_remote_copy(
+            src_ref=ends.at[s], dst_ref=ends.at[s], send_sem=esend.at[j - 1], recv_sem=erecv.at[j - 1],
+            device_id=(lax.rem(s + j, n), t), device_id_type=MESH)
+
+    def end_arrived(j):
+        o = lax.rem(s + n - j, n)
+        pltpu.make_async_remote_copy(
+            src_ref=ends.at[o], dst_ref=ends.at[o], send_sem=esend.at[j - 1], recv_sem=erecv.at[j - 1],
+            device_id=(lax.rem(s + j, n), t), device_id_type=MESH).wait_recv()
+
+    for j in range(1, n):
+        end_copy(j).start()
+    relay(0, 1)
+    for j in range(1, n):
+        end_arrived(j)
+    carry = jnp.zeros((8, loc), F32)
+    for o in range(n - 1):
+        e = ends[o]
+        carry = jnp.where(o < s, e[:8] * carry + e[8:], carry)
+    cin = carry[0:1]
+
+    def branch(i, _):
+        r = pl.multiple_of(i * CH, CH)
+        st = drv[pl.ds(r, CH)] + fac[pl.ds(r, CH)] * cin
+        bfull[t, pl.ds(r, CH)] = (st * jax.nn.gelu(gate_branch[pl.ds(r, CH)].astype(F32))).astype(BF16)
+        return 0
+
+    lax.fori_loop(0, tok // CH, branch, 0)
+
+    def tp_push(view, send, recv, j, start):
+        o = t if start else lax.rem(t + ntp - j, ntp)
+        return pltpu.make_async_remote_copy(
+            src_ref=view(o), dst_ref=view(o), send_sem=send.at[j - 1], recv_sem=recv.at[j - 1],
+            device_id=(s, lax.rem(t + j, ntp)), device_id_type=MESH)
+
+    def bview(o):
+        return bfull.at[o]
+
+    chips = ntp // 2
+    core = lax.rem(t, 2)
+    mate = t + 1 - 2 * core
+
+    def far(view, send, recv, c, start):
+        o = t if start else lax.rem(t + ntp - 2 * c, ntp)
+        return pltpu.make_async_remote_copy(
+            src_ref=view(o), dst_ref=view(o), send_sem=send.at[c - 1], recv_sem=recv.at[c - 1],
+            device_id=(s, lax.rem(t + 2 * c, ntp)), device_id_type=MESH)
+
+    def near(view, send, recv, c, start):
+        base = t if start else mate
+        o = lax.rem(base + ntp - 2 * c, ntp)
+        return pltpu.make_async_remote_copy(
+            src_ref=view(o), dst_ref=view(o), send_sem=send.at[chips - 1 + c], recv_sem=recv.at[chips - 1 + c],
+            device_id=(s, mate), device_id_type=MESH)
+
+    def gather_start(view, send, recv):
+        for c in range(1, chips):
+            far(view, send, recv, c, True).start()
+        near(view, send, recv, 0, True).start()
+
+    def gather_share(view, send, recv):
+        for c in range(1, chips):
+            far(view, send, recv, c, False).wait_recv()
+            near(view, send, recv, c, True).start()
+
+    def gather_wait(view, send, recv):
+        for c in range(chips):
+            near(view, send, recv, c, False).wait_recv()
+
+    def gather_sent(view, send, recv):
+        for c in range(1, chips):
+            far(view, send, recv, c, True).wait_send()
+        for c in range(chips):
+            near(view, send, recv, c, True).wait_send()
+
+    gather_start(bview, bsend, brecv)
+    relay(1, 1)
+    gather_share(bview, bsend, brecv)
+    gather_wait(bview, bsend, brecv)
+
+    def row_total(q, values):
+        def write(i, _):
+            r = pl.multiple_of(i * BR, BR)
+            v = values(r)
+            c = jnp.sum(v * v, axis=1, keepdims=True)
+            ssq[q, t, :, pl.ds(r, BR)] = jnp.transpose(jnp.broadcast_to(c, (BR, 128)))[:8]
+            return 0
+
+        lax.fori_loop(0, tok // BR, write, 0)
+        for j in range(1, ntp):
+            tp_push(lambda o: ssq.at[q, o], qsend.at[q], qrecv.at[q], j, True).start()
+
+    def wait_total(q):
+        for j in range(1, ntp):
+            tp_push(lambda o: ssq.at[q, o], qsend.at[q], qrecv.at[q], j, False).wait_recv()
+
+    def inverse_rms(q, r):
+        row = ssq[q, 0, 0:1, pl.ds(r, BR)]
+        for o in range(1, ntp):
+            row = row + ssq[q, o, 0:1, pl.ds(r, BR)]
+        inv = lax.rsqrt(row / width + EPS)
+        return jnp.transpose(jnp.broadcast_to(inv, (128, BR)))[:, 0:1]
+
+    def project(i, _):
+        r = pl.multiple_of(i * BR, BR)
+        total = jnp.zeros((BR, dloc), F32)
+        for o in range(ntp):
+            total += jnp.dot(bfull[o, pl.ds(r, BR)], out_w[pl.ds(o * loc, loc)], preferred_element_type=F32)
+        mixed[pl.ds(r, BR)] = total.astype(BF16)
+        return 0
+
+    lax.fori_loop(0, tok // BR, project, 0)
+    row_total(0, lambda r: mixed[pl.ds(r, BR)].astype(F32))
+    wait_total(0)
+
+    def stream(i, _):
+        r = pl.multiple_of(i * BR, BR)
+        m = mixed[pl.ds(r, BR)].astype(F32)
+        mixed[pl.ds(r, BR)] = (residual[pl.ds(r, BR)].astype(F32) + m * inverse_rms(0, r) * mix_gain[...]).astype(BF16)
+        return 0
+
+    lax.fori_loop(0, tok // BR, stream, 0)
+    row_total(1, lambda r: mixed[pl.ds(r, BR)].astype(F32))
+    relay(0, 2)
+    wait_total(1)
+
+    cols = pl.ds(pl.multiple_of(t * dloc, dloc), dloc)
+
+    def norm(i, _):
+        r = pl.multiple_of(i * BR, BR)
+        m = mixed[pl.ds(r, BR)].astype(F32)
+        v = (m * inverse_rms(1, r) * pre_gain[...]).astype(BF16)
+        nloc[pl.ds(r, BR)] = v
+
+        @pl.when(y == core)
+        def _():
+            normed[pl.ds(r, BR), cols] = v
+
+        return 0
+
+    lax.fori_loop(0, tok // BR, norm, 0)
+
+    def n_copy(dy, dx):
+        return pltpu.make_async_remote_copy(
+            src_ref=nloc, dst_ref=normed.at[:, cols], send_sem=nsend.at[dy, dx], recv_sem=nrecv.at[t],
+            device_id=(z * ny + lax.rem(y + dy, ny), 2 * lax.rem(x + dx, chips) + y), device_id_type=MESH)
+
+    def to_plane(act):
+        for dy in range(ny):
+            for dx in range(chips):
+                if dy or dx:
+                    act(n_copy(dy, dx))
+                else:
+                    @pl.when(y != core)
+                    def _():
+                        act(n_copy(0, 0))
+
+    def n_wait(dt):
+        o = lax.rem(t + dt, ntp)
+        view = normed.at[:, pl.ds(pl.multiple_of(o * dloc, dloc), dloc)]
+        pltpu.make_async_remote_copy(
+            src_ref=view, dst_ref=view, send_sem=nsend.at[0, 0], recv_sem=nrecv.at[o],
+            device_id=(s, mate), device_id_type=MESH).wait_recv()
+
+    to_plane(start)
+    relay(1, 2)
+    ends_line = jnp.logical_or(z == 0, z == nz - 1)
+
+    @pl.when(ends_line)
+    def _():
+        push_seed(2)
+
+    for j in range(3, nz):
+        relay(0, j)
+        relay(1, j)
+
+    @pl.when(jnp.logical_not(ends_line))
+    def _():
+        push_seed(2)
+
+    for dt in range(1, ntp):
+        n_wait(dt)
+
+    @pl.when(y != core)
+    def _():
+        n_wait(0)
+
+    for a in range(2):
+        for o in range(nz):
+            mate_copy(a, o, True).wait_recv()
+
+    def ffn_tile(c, size):
+        cs = pl.ds(c, size)
+        g = jnp.dot(normed[...], gate_all[:, cs], preferred_element_type=F32)
+        u = jnp.dot(normed[...], up_all[:, cs], preferred_element_type=F32)
+        hidden[:, cs] = (jax.nn.silu(g) * u).astype(BF16)
+
+    TN = 256
+    tiles = ff // TN
+
+    def ffn_step(j, _):
+        ffn_tile(pl.multiple_of(j * TN, TN), TN)
+        return 0
+
+    lax.fori_loop(0, tiles, ffn_step, 0)
+    if ff % TN:
+        ffn_tile(tiles * TN, ff % TN)
+
+    me = y * chips + x
+
+    def p_copy(i):
+        return pltpu.make_async_remote_copy(
+            src_ref=partial.at[i], dst_ref=recvd.at[me, lax.rem(i, per)], send_sem=psend.at[i],
+            recv_sem=precv.at[me, lax.rem(i, per)],
+            device_id=(z * ny + core, lax.div(i, per)), device_id_type=MESH)
+
+    def owned(i):
+        return jnp.logical_and(y == core, lax.div(i, per) == t)
+
+    for j in range(nz):
+        o = origin[j]
+        if j:
+            relay(2, j)
+        for b in range(ny):
+            @pl.when(b != core)
+            def _():
+                mate_copy(2, o, True).wait_recv()
+
+            i = o * ny + b
+            partial[i] = jnp.dot(hidden[...], down_all[i], preferred_element_type=F32).astype(BF16)
+
+            @pl.when(owned(i))
+            def _():
+                recvd[me, lax.rem(i, per)] = partial[i]
+
+            @pl.when(jnp.logical_not(owned(i)))
+            def _():
+                p_copy(i).start()
+
+    def p_wait(dy, dx):
+        k = lax.rem(y + dy, ny) * chips + lax.rem(x + dx, chips)
+        for w in range(per):
+            pltpu.make_async_remote_copy(
+                src_ref=partial.at[0], dst_ref=recvd.at[k, w], send_sem=psend.at[0], recv_sem=precv.at[k, w],
+                device_id=(s, mate), device_id_type=MESH).wait_recv()
+
+    for dy in range(ny):
+        for dx in range(chips):
+            if dy or dx:
+                p_wait(dy, dx)
+
+    @pl.when(y != core)
+    def _():
+        p_wait(0, 0)
+
+    def gather_sum(i, _):
+        r = pl.multiple_of(i * BR, BR)
+        for w in range(per):
+            total = recvd[0, w, pl.ds(r, BR)].astype(F32)
+            for k in range(1, ny * chips):
+                total = total + recvd[k, w, pl.ds(r, BR)].astype(F32)
+            out[pl.ds(r, BR), pl.ds(w * ncol, ncol)] = total.astype(BF16)
+        return 0
+
+    lax.fori_loop(0, tok // BR, gather_sum, 0)
+    row_total(2, lambda r: out[pl.ds(r, BR)].astype(F32))
+    wait_total(2)
+
+    def finish(i, _):
+        r = pl.multiple_of(i * BR, BR)
+        f = out[pl.ds(r, BR)].astype(F32)
+        out[pl.ds(r, BR)] = (mixed[pl.ds(r, BR)].astype(F32) + f * inverse_rms(2, r) * ffn_gain[...]).astype(BF16)
+        return 0
+
+    lax.fori_loop(0, tok // BR, finish, 0)
+
+    def sent(c):
+        c.wait_send()
+
+    for a in range(3):
+        @pl.when(y != core)
+        def _():
+            seed_swap(a).wait_send()
+
+        for j in range(nz):
+            fan(a, origin[j], sent)
+    for j in range(1, n):
+        end_copy(j).wait_send()
+    gather_sent(bview, bsend, brecv)
+    to_plane(sent)
+    for i in range(n):
+        @pl.when(jnp.logical_not(owned(i)))
+        def _():
+            p_copy(i).wait_send()
+    for j in range(1, ntp):
+        for q in range(3):
+            tp_push(lambda o: ssq.at[q, o], qsend.at[q], qrecv.at[q], j, True).wait_send()
+
+
 def body(n, ntp, gate_branch, recur_input, doc_ids, conv_taps, gate_map, input_map, decay_level, decay_extra,
          out_weight, residual, mix_gain, pre_gain, ffn_gain, gate_weight, up_weight, down_weight):
     tok, loc = recur_input.shape
@@ -518,12 +1028,21 @@
     V, S = pltpu.VMEM, pltpu.SemaphoreType.DMA
     per = dloc // ncol
     chips = ntp // 2
-    return pl.pallas_call(
-        functools.partial(kernel, (n, ntp, nz, ny, dloc * ntp)),
-        out_shape=jax.ShapeDtypeStruct((tok, dloc), BF16),
-        in_specs=[vm] * 13 + [hbm] * 3,
-        out_specs=vm,
-        scratch_shapes=[
+    if ny == 2:
+        fn = plane_kernel
+        scratch = [
+            V((n * krows, ff), BF16), V((n * krows, ff), BF16), V((n, ff, ncol), BF16),
+            V((tok + 8, loc), F32), V((tok + 8, 128), jnp.int32), V((16, loc), BF16), V((8, 128), jnp.int32),
+            V((2, loc, loc), BF16), V((tok, loc), F32), V((tok, loc), F32), V((n, 16, loc), F32),
+            V((ntp, tok, loc), BF16), V((tok, dloc), BF16), V((tok, dloc), BF16), V((tok, dloc * ntp), BF16),
+            V((tok, ff), BF16), V((n, tok, ncol), BF16), V((ny * chips, per, tok, ncol), BF16), V((3, ntp, 8, tok), F32),
+            S((3,)), S((3,)), S((3,)), S((2, 3, nz)), S((3, nz)), S((3, nz)), S((3, nz)),
+            S((2,)), S((2,)), S((n - 1,)), S((n - 1,)), S((ntp - 1,)), S((ntp - 1,)),
+            S((ny, chips)), S((ntp,)), S((3, ntp - 1)), S((3, ntp - 1)), S((n,)), S((ny * chips, per)),
+        ]
+    else:
+        fn = kernel
+        scratch = [
             V((n * krows, ff), BF16), V((n * krows, ff), BF16), V((n, ff, ncol), BF16),
             V((tok + 8, loc), F32), V((tok + 8, 128), jnp.int32), V((16, loc), BF16), V((8, 128), jnp.int32),
             V((2, loc, loc), BF16), V((tok, loc), F32), V((tok, loc), F32), V((n, 16, loc), F32),
@@ -533,7 +1052,13 @@
             S((3, 2, n - 1)), S((3, 2, n - 1)), S((3,)), S((2,)), S((2,)), S((n - 1,)), S((n - 1,)),
             S((ntp - 1,)), S((ntp - 1,)), S((ntp - 1,)), S((ntp - 1,)), S((3, ntp - 1)), S((3, ntp - 1)),
             S((n,)), S((chips - 1, per)), S((n,)),
-        ],
+        ]
+    return pl.pallas_call(
+        functools.partial(fn, (n, ntp, nz, ny, dloc * ntp)),
+        out_shape=jax.ShapeDtypeStruct((tok, dloc), BF16),
+        in_specs=[vm] * 13 + [hbm] * 3,
+        out_specs=vm,
+        scratch_shapes=scratch,
         compiler_params=pltpu.CompilerParams(
             collective_id=0, has_side_effects=True, vmem_limit_bytes=62 * 1024 * 1024),
     )(*args)

time: 211 us -> 199 us (0.943); the launches traced: 207 us -> 198 us
  Pallas kernels: 202 us -> 193 us
    pallas_call x1, Pallas kernels: 202 us -> 193 us  [body(): pl.pallas_call(functools.partial(fn, (n, ntp, nz, ny, dloc * ntp)), out_s...]
where the time goes in v1:
time: 199 us; the launch traced here: 198 us
  Pallas kernels  193 us (97%)
  local copies, waits for them, and re-layouts  3.77 us (2%)
    pallas_call x1, Pallas kernels, body(): pl.pallas_call(functools.partial(fn, (n, ntp, nz, ny, dloc * ntp)), out_s...  193 us

profile of v1, /device:TPU:0, one launch (start us, length us, event | category | flops | bytes accessed | tf_op | source)
XLA Modules:
  0.0 198.4 jit_solution(9708359315260970870)
XLA Ops:
  0.0 0.0 copy-start.2
  0.0 0.7 copy-done.2
  0.7 0.0 copy-start.1
  0.7 0.6 fusion.1
  1.2 0.0 copy-start
  1.2 0.1 copy-done.1
  1.4 0.6 convert_element_type.3.taps
  1.9 0.0 copy-done
  2.0 0.9 broadcast_in_dim.18.ids
  2.9 193.4 %shard_map.154 = bf16[768,512]{1,0:T(8,128)(2,1)} custom-call(bf16[768,256]{1,0:T(8,128)(2,1)} %gate_branch.1, bf16[768,256]{1,0:T(8,128)(2,1)} %recur.1, s32[768,128]{1,0:T(8,128)} %broadcast_in_dim.18.ids, f32[4,256]{1,0:T(4,128)} %convert_element_type.3.taps, bf16[256,64]{1,0:T(8,128)(2,1)} %bitcast.6, bf16[256,64]{1,0:T(8,128)(2,1)} %bitcast.7, ...), custom_call_target="tpu_custom_call" | custom-call | tf_op jit(solution)/shard_map/pallas_call | solution.py:1056
  196.3 2.1 %copy.18 = bf16[768,512]{1,0:T(8,128)(2,1)} copy(bf16[768,512]{1,0:T(8,128)(2,1)} %shard_map.154) | data formatting | bytes 1572864
Async XLA Ops:
  0.0 0.7 copy-start.2
  0.7 0.7 copy-start.1
  1.2 0.7 copy-start

commit v2 on v1

--- a/solution.py
+++ b/solution.py
@@ -506,7 +506,7 @@
     mix_gain, pre_gain, ffn_gain, gate_w, up_w, down_w,
     out,
     gate_all, up_all, down_all, xpad, idpad, halo, ihalo, bd, fac, drv, ends, bfull,
-    mixed, nloc, normed, hidden, partial, recvd, ssq,
+    mixed, nloc, normed, gsum, usum, hidden, partial, recvd, ssq,
     lsem, ssend, srecv, zsend, zrecv, msend, mrecv,
     hsend, hrecv, esend, erecv, bsend, brecv, nsend, nrecv, qsend, qrecv, psend, precv,
 ):
@@ -532,8 +532,6 @@
         pl.semaphore_signal(barrier, inc=1, device_id=p, device_id_type=MESH)
     pl.semaphore_wait(barrier, len(peers))
 
-    shard = (gate_w, up_w, down_w)
-    whole = (gate_all, up_all, down_all)
     low = (2 * z < nz).astype(jnp.int32)
     near_first = []
     for k in range(1, nz):
@@ -548,18 +546,31 @@
     for j in range(1, nz):
         origin.append(sum(jnp.where(jnp.logical_and(ok == 1, r == j), q, 0) for q, ok, r in ranks))
 
+    hcol = ncol // 2
+    hrow = krows // 2
+    GATE, UP, DOWN = (0, 1), (2,), (3, 4)
+
     def block(a, o, b):
         i = o * ny + b
-        if a < 2:
-            return whole[a].at[pl.ds(pl.multiple_of(i * krows, krows), krows)]
-        return whole[a].at[i]
+        if a in GATE:
+            return gate_all.at[pl.ds(pl.multiple_of(i * krows + a * hrow, hrow), hrow)]
+        if a in UP:
+            return up_all.at[pl.ds(pl.multiple_of(i * krows, krows), krows)]
+        return down_all.at[i, :, pl.ds((a - DOWN[0]) * hcol, hcol)]
+
+    def own_shard(a):
+        if a in GATE:
+            return gate_w.at[pl.ds(a * hrow, hrow)]
+        if a in UP:
+            return up_w
+        return down_w.at[:, pl.ds((a - DOWN[0]) * hcol, hcol)]
 
     def seed_local(a):
-        return pltpu.make_async_copy(shard[a], block(a, z, y), lsem.at[a])
+        return pltpu.make_async_copy(own_shard(a), block(a, z, y), lsem.at[a])
 
     def seed_swap(a):
         return pltpu.make_async_remote_copy(
-            src_ref=shard[a], dst_ref=block(a, z, y), send_sem=ssend.at[a], recv_sem=srecv.at[a],
+            src_ref=own_shard(a), dst_ref=block(a, z, y), send_sem=ssend.at[a], recv_sem=srecv.at[a],
             device_id=(z * ny + 1 - y, mate), device_id_type=MESH)
 
     def z_copy(a, o, up):
@@ -592,7 +603,7 @@
     def start(c):
         c.start()
 
-    def push_seed(a):
+    def seed_ready(a):
         @pl.when(y == core)
         def _():
             seed_local(a).wait()
@@ -603,14 +614,19 @@
                 src_ref=block(a, z, core), dst_ref=block(a, z, core), send_sem=ssend.at[a], recv_sem=srecv.at[a],
                 device_id=(z * ny + 1 - y, mate), device_id_type=MESH).wait_recv()
 
+    def push_seed(a):
+        seed_ready(a)
         fan(a, z, start)
 
-    def relay(a, j):
-        o = origin[j]
+    def relay_from(a, o):
         z_copy(a, o, 0).wait_recv()
         fan(a, o, start)
 
-    for a in range(3):
+    def relay(items, j):
+        for a in items:
+            relay_from(a, origin[j])
+
+    def load_seed(a):
         @pl.when(y == core)
         def _():
             seed_local(a).start()
@@ -628,10 +644,13 @@
     for i in range(2):
         halo_copy(i).start()
 
+    for a in GATE:
+        load_seed(a)
+
     @pl.when(y == core)
     def _():
-        push_seed(0)
-        push_seed(1)
+        for a in GATE:
+            push_seed(a)
 
     head = gmap.shape[1]
     spread = (lax.rem(lax.broadcasted_iota(jnp.int32, (head, loc), 1), head)
@@ -655,10 +674,6 @@
         return 0
 
     lax.fori_loop(0, tok // CH, fill, 0)
-
-    @pl.when(y != core)
-    def _():
-        push_seed(0)
 
     reps = loc // 128
     ntaps = taps.shape[0]
@@ -687,9 +702,13 @@
 
     lax.fori_loop(0, tok // CH, front, 0)
 
+    @pl.when(y == core)
+    def _():
+        load_seed(UP[0])
+
     @pl.when(y != core)
     def _():
-        push_seed(1)
+        push_seed(GATE[0])
 
     rows8 = lax.broadcasted_iota(jnp.int32, (8, loc), 0)
 
@@ -723,7 +742,21 @@
 
     for j in range(1, n):
         end_copy(j).start()
-    relay(0, 1)
+
+    @pl.when(y != core)
+    def _():
+        load_seed(UP[0])
+        push_seed(GATE[1])
+
+    for a in DOWN:
+        load_seed(a)
+
+    @pl.when(y == core)
+    def _():
+        push_seed(UP[0])
+
+    inner = jnp.logical_and(z > 0, z < nz - 1)
+    early = min(2, nz - 1)
     for j in range(1, n):
         end_arrived(j)
     carry = jnp.zeros((8, loc), F32)
@@ -787,7 +820,16 @@
             near(view, send, recv, c, True).wait_send()
 
     gather_start(bview, bsend, brecv)
-    relay(1, 1)
+
+    @pl.when(y != core)
+    def _():
+        push_seed(UP[0])
+
+    @pl.when(inner)
+    def _():
+        for j in range(1, early + 1):
+            relay(GATE, j)
+
     gather_share(bview, bsend, brecv)
     gather_wait(bview, bsend, brecv)
 
@@ -824,6 +866,12 @@
 
     lax.fori_loop(0, tok // BR, project, 0)
     row_total(0, lambda r: mixed[pl.ds(r, BR)].astype(F32))
+
+    @pl.when(inner)
+    def _():
+        for j in range(1, early + 1):
+            relay(UP, j)
+
     wait_total(0)
 
     def stream(i, _):
@@ -834,7 +882,6 @@
 
     lax.fori_loop(0, tok // BR, stream, 0)
     row_total(1, lambda r: mixed[pl.ds(r, BR)].astype(F32))
-    relay(0, 2)
     wait_total(1)
 
     cols = pl.ds(pl.multiple_of(t * dloc, dloc), dloc)
@@ -876,86 +923,174 @@
             device_id=(s, mate), device_id_type=MESH).wait_recv()
 
     to_plane(start)
-    relay(1, 2)
-    ends_line = jnp.logical_or(z == 0, z == nz - 1)
-
-    @pl.when(ends_line)
+
+    @pl.when(jnp.logical_not(inner))
     def _():
-        push_seed(2)
-
-    for j in range(3, nz):
-        relay(0, j)
-        relay(1, j)
-
-    @pl.when(jnp.logical_not(ends_line))
-    def _():
-        push_seed(2)
-
-    for dt in range(1, ntp):
-        n_wait(dt)
-
-    @pl.when(y != core)
-    def _():
-        n_wait(0)
-
-    for a in range(2):
-        for o in range(nz):
-            mate_copy(a, o, True).wait_recv()
-
-    def ffn_tile(c, size):
-        cs = pl.ds(c, size)
-        g = jnp.dot(normed[...], gate_all[:, cs], preferred_element_type=F32)
-        u = jnp.dot(normed[...], up_all[:, cs], preferred_element_type=F32)
-        hidden[:, cs] = (jax.nn.silu(g) * u).astype(BF16)
-
+        for a in DOWN:
+            push_seed(a)
+        for j in range(1, early + 1):
+            relay(GATE, j)
+            relay(UP, j)
+
+    def outward_seed():
+        for a in DOWN:
+            @pl.when(low == 1)
+            def _():
+                fan_down(a, z, start)
+
+            @pl.when(low == 0)
+            def _():
+                fan_up(a, z, start)
+
+    def mates(js):
+        for j in js:
+            for a in GATE + UP:
+                mate_copy(a, origin[j], True).wait_recv()
+
+    def n_ready():
+        for dt in range(1, ntp):
+            n_wait(dt)
+
+        @pl.when(y != core)
+        def _():
+            n_wait(0)
+
+    kblk = ny * krows
     TN = 256
     tiles = ff // TN
 
-    def ffn_step(j, _):
-        ffn_tile(pl.multiple_of(j * TN, TN), TN)
-        return 0
-
-    lax.fori_loop(0, tiles, ffn_step, 0)
-    if ff % TN:
-        ffn_tile(tiles * TN, ff % TN)
+    def sums(js, cs):
+        g = u = None
+        for j in js:
+            k = pl.ds(pl.multiple_of(origin[j] * kblk, kblk), kblk)
+            a = normed[:, k]
+            gj = jnp.dot(a, gate_all[k, cs], preferred_element_type=F32)
+            uj = jnp.dot(a, up_all[k, cs], preferred_element_type=F32)
+            g, u = (gj, uj) if g is None else (g + gj, u + uj)
+        return g, u
+
+    def first_tile(c, size):
+        cs = pl.ds(c, size)
+        gsum[:, cs], usum[:, cs] = sums(range(nz - 1), cs)
+
+    def last_tile(c, size):
+        cs = pl.ds(c, size)
+        g, u = sums((nz - 1,), cs)
+        g, u = g + gsum[:, cs], u + usum[:, cs]
+        hidden[:, cs] = (jax.nn.silu(g) * u).astype(BF16)
+
+    def over_tiles(tile):
+        def step(j, _):
+            tile(pl.multiple_of(j * TN, TN), TN)
+            return 0
+
+        lax.fori_loop(0, tiles, step, 0)
+        if ff % TN:
+            tile(tiles * TN, ff % TN)
+
+    @pl.when(inner)
+    def _():
+        for j in range(early + 1, nz):
+            relay(GATE, j)
+            relay(UP, j)
+        for a in DOWN:
+            seed_ready(a)
+            mate_copy(a, z).start()
+
+            @pl.when(low == 1)
+            def _():
+                fan_up(a, z, start)
+
+            @pl.when(low == 0)
+            def _():
+                fan_down(a, z, start)
+
+        @pl.when(core == 0)
+        def _():
+            outward_seed()
+
+    n_ready()
+    mates(range(nz - 1))
+    over_tiles(first_tile)
+
+    @pl.when(jnp.logical_not(inner))
+    def _():
+        for j in range(early + 1, nz):
+            relay(GATE, j)
+            relay(UP, j)
+
+    mates((nz - 1,))
+    over_tiles(last_tile)
 
     me = y * chips + x
 
-    def p_copy(i):
-        return pltpu.make_async_remote_copy(
-            src_ref=partial.at[i], dst_ref=recvd.at[me, lax.rem(i, per)], send_sem=psend.at[i],
-            recv_sem=precv.at[me, lax.rem(i, per)],
+    def p_copy(i, h):
+        c = pl.ds(h * hcol, hcol)
+        return pltpu.make_async_remote_copy(
+            src_ref=partial.at[i, :, c], dst_ref=recvd.at[me, lax.rem(i, per), :, c], send_sem=psend.at[i, h],
+            recv_sem=precv.at[me, lax.rem(i, per), h],
             device_id=(z * ny + core, lax.div(i, per)), device_id_type=MESH)
 
     def owned(i):
         return jnp.logical_and(y == core, lax.div(i, per) == t)
 
+    def ship(i, hs):
+        @pl.when(owned(i))
+        def _():
+            for h in hs:
+                c = pl.ds(h * hcol, hcol)
+                recvd[me, lax.rem(i, per), :, c] = partial[i, :, c]
+
+        @pl.when(jnp.logical_not(owned(i)))
+        def _():
+            for h in hs:
+                p_copy(i, h).start()
+
+    def mate_ready(a, o, b):
+        @pl.when(b != core)
+        def _():
+            mate_copy(a, o, True).wait_recv()
+
+    def order(b, j):
+        if b == 0 or j == 0:
+            return origin[j]
+        return jnp.where(inner, origin[j], origin[1 + j % (nz - 1)])
+
     for j in range(nz):
-        o = origin[j]
-        if j:
-            relay(2, j)
-        for b in range(ny):
-            @pl.when(b != core)
-            def _():
-                mate_copy(2, o, True).wait_recv()
-
-            i = o * ny + b
-            partial[i] = jnp.dot(hidden[...], down_all[i], preferred_element_type=F32).astype(BF16)
-
-            @pl.when(owned(i))
-            def _():
-                recvd[me, lax.rem(i, per)] = partial[i]
-
-            @pl.when(jnp.logical_not(owned(i)))
-            def _():
-                p_copy(i).start()
+        mine = jnp.where(core == 0, order(0, j), order(1, j))
+        if j < nz - 1:
+            if j:
+                for a in DOWN:
+                    relay_from(a, mine)
+            for b in range(ny):
+                i = order(b, j) * ny + b
+                for a in DOWN:
+                    mate_ready(a, order(b, j), b)
+                partial[i] = jnp.dot(hidden[...], down_all[i], preferred_element_type=F32).astype(BF16)
+                ship(i, (0, 1))
+        else:
+            for h in range(2):
+                relay_from(DOWN[h], mine)
+                if h == 1:
+                    @pl.when(jnp.logical_and(inner, core == 1))
+                    def _():
+                        outward_seed()
+
+                c = pl.ds(h * hcol, hcol)
+                for b in range(ny):
+                    i = order(b, j) * ny + b
+                    mate_ready(DOWN[h], order(b, j), b)
+                    partial[i, :, c] = jnp.dot(hidden[...], down_all[i, :, c], preferred_element_type=F32).astype(BF16)
+                    ship(i, (h,))
 
     def p_wait(dy, dx):
         k = lax.rem(y + dy, ny) * chips + lax.rem(x + dx, chips)
         for w in range(per):
-            pltpu.make_async_remote_copy(
-                src_ref=partial.at[0], dst_ref=recvd.at[k, w], send_sem=psend.at[0], recv_sem=precv.at[k, w],
-                device_id=(s, mate), device_id_type=MESH).wait_recv()
+            for h in range(2):
+                view = recvd.at[k, w, :, pl.ds(h * hcol, hcol)]
+                pltpu.make_async_remote_copy(
+                    src_ref=view, dst_ref=view, send_sem=psend.at[0, 0], recv_sem=precv.at[k, w, h],
+                    device_id=(s, mate), device_id_type=MESH).wait_recv()
 
     for dy in range(ny):
         for dx in range(chips):
@@ -990,7 +1125,7 @@
     def sent(c):
         c.wait_send()
 
-    for a in range(3):
+    for a in GATE + UP + DOWN:
         @pl.when(y != core)
         def _():
             seed_swap(a).wait_send()
@@ -1004,7 +1139,8 @@
     for i in range(n):
         @pl.when(jnp.logical_not(owned(i)))
         def _():
-            p_copy(i).wait_send()
+            for h in range(2):
+                p_copy(i, h).wait_send()
     for j in range(1, ntp):
         for q in range(3):
             tp_push(lambda o: ssq.at[q, o], qsend.at[q], qrecv.at[q], j, True).wait_send()
@@ -1035,10 +1171,10 @@
             V((tok + 8, loc), F32), V((tok + 8, 128), jnp.int32), V((16, loc), BF16), V((8, 128), jnp.int32),
             V((2, loc, loc), BF16), V((tok, loc), F32), V((tok, loc), F32), V((n, 16, loc), F32),
             V((ntp, tok, loc), BF16), V((tok, dloc), BF16), V((tok, dloc), BF16), V((tok, dloc * ntp), BF16),
-            V((tok, ff), BF16), V((n, tok, ncol), BF16), V((ny * chips, per, tok, ncol), BF16), V((3, ntp, 8, tok), F32),
-            S((3,)), S((3,)), S((3,)), S((2, 3, nz)), S((3, nz)), S((3, nz)), S((3, nz)),
+            V((tok, ff), F32), V((tok, ff), F32), V((tok, ff), BF16), V((n, tok, ncol), BF16), V((ny * chips, per, tok, ncol), BF16), V((3, ntp, 8, tok), F32),
+            S((5,)), S((5,)), S((5,)), S((2, 5, nz)), S((5, nz)), S((5, nz)), S((5, nz)),
             S((2,)), S((2,)), S((n - 1,)), S((n - 1,)), S((ntp - 1,)), S((ntp - 1,)),
-            S((ny, chips)), S((ntp,)), S((3, ntp - 1)), S((3, ntp - 1)), S((n,)), S((ny * chips, per)),
+            S((ny, chips)), S((ntp,)), S((3, ntp - 1)), S((3, ntp - 1)), S((n, 2)), S((ny * chips, per, 2)),
         ]
     else:
         fn = kernel

time: 199 us -> 181 us (0.910)
  the two profiles are of different devices: /device:TPU:0 before, /device:TPU:5 now
where the time goes in v2:
time: 181 us
  Pallas kernels  176 us (97%)
  local copies, waits for them, and re-layouts  3.77 us (2%)
    pallas_call x1, Pallas kernels, body(): pl.pallas_call(functools.partial(fn, (n, ntp, nz, ny, dloc * ntp)), out_s...  176 us

profile of v2, /device:TPU:5, one launch (start us, length us, event | category | flops | bytes accessed | tf_op | source)
XLA Modules:
  0.0 181.2 jit_solution(9935856882097301462)
XLA Ops:
  0.0 0.0 copy-start.2
  0.0 0.7 copy-done.2
  0.7 0.0 copy-start.1
  0.7 0.6 fusion.1
  1.2 0.0 copy-start
  1.2 0.1 copy-done.1
  1.4 0.6 convert_element_type.3.taps
  1.9 0.0 copy-done
  2.0 0.9 broadcast_in_dim.18.ids
  2.9 176.3 %shard_map.154 = bf16[768,512]{1,0:T(8,128)(2,1)} custom-call(bf16[768,256]{1,0:T(8,128)(2,1)} %gate_branch.1, bf16[768,256]{1,0:T(8,128)(2,1)} %recur.1, s32[768,128]{1,0:T(8,128)} %broadcast_in_dim.18.ids, f32[4,256]{1,0:T(4,128)} %convert_element_type.3.taps, bf16[256,64]{1,0:T(8,128)(2,1)} %bitcast.6, bf16[256,64]{1,0:T(8,128)(2,1)} %bitcast.7, ...), custom_call_target="tpu_custom_call" | custom-call | tf_op jit(solution)/shard_map/pallas_call | solution.py:1192
  179.2 2.1 %copy.18 = bf16[768,512]{1,0:T(8,128)(2,1)} copy(bf16[768,512]{1,0:T(8,128)(2,1)} %shard_map.154) | data formatting | bytes 1572864
Async XLA Ops:
  0.0 0.7 copy-start.2
  0.7 0.7 copy-start.1
  1.2 0.7 copy-start

commit v3 on v2

--- a/solution.py
+++ b/solution.py
@@ -502,9 +502,10 @@
 
 def plane_kernel(
     cfg,
-    gate_branch, recur, ids, taps, gmap, imap, rate, extra, out_w, residual,
+    gate_branch_in, recur_in, ids, taps, gmap, imap, level, extra_in, out_w_in, residual_in,
     mix_gain, pre_gain, ffn_gain, gate_w, up_w, down_w,
-    out,
+    out_hbm,
+    out, osem, gate_branch, recur, extra, out_w, residual, insem,
     gate_all, up_all, down_all, xpad, idpad, halo, ihalo, bd, fac, drv, ends, bfull,
     mixed, nloc, normed, gsum, usum, hidden, partial, recvd, ssq,
     lsem, ssend, srecv, zsend, zrecv, msend, mrecv,
@@ -530,6 +531,14 @@
     peers += [(lax.rem(z + dz, nz) * ny + lax.rem(y + dy, ny), t) for dz in range(1, nz) for dy in range(ny)]
     for p in peers:
         pl.semaphore_signal(barrier, inc=1, device_id=p, device_id_type=MESH)
+
+    inputs = ((recur_in, recur), (extra_in, extra), (gate_branch_in, gate_branch), (out_w_in, out_w), (residual_in, residual))
+
+    def load_input(i):
+        return pltpu.make_async_copy(inputs[i][0], inputs[i][1], insem.at[i])
+
+    for i in range(len(inputs)):
+        load_input(i).start()
     pl.semaphore_wait(barrier, len(peers))
 
     low = (2 * z < nz).astype(jnp.int32)
@@ -636,7 +645,7 @@
             seed_swap(a).start()
 
     def halo_copy(i):
-        src, dst = ((recur.at[pl.ds(tok - 16, 16)], halo), (ids.at[pl.ds(tok - 8, 8)], ihalo))[i]
+        src, dst = ((recur_in.at[pl.ds(tok - 16, 16)], halo), (ids, ihalo))[i]
         return pltpu.make_async_remote_copy(
             src_ref=src, dst_ref=dst, send_sem=hsend.at[i], recv_sem=hrecv.at[i],
             device_id=(lax.rem(s + 1, n), t), device_id_type=MESH)
@@ -662,19 +671,27 @@
         bd[i] = jnp.where(diag, tiled, 0.0).astype(BF16)
 
     for i in range(2):
+        load_input(i).wait()
+
+    def down_rows(row):
+        return jnp.transpose(jnp.broadcast_to(row, (128, 128)))
+
+    for i in range(tok // 128):
+        idpad[pl.ds(8 + i * 128, 128)] = down_rows(ids[i:i + 1])
+
+    def fill(i, _):
+        r = pl.multiple_of(i * CH, CH)
+        xpad[pl.ds(pl.multiple_of(r + 8, 8), CH)] = recur[pl.ds(r, CH)].astype(F32)
+        return 0
+
+    lax.fori_loop(0, tok // CH, fill, 0)
+    u = -level[...]
+    rate = -GATE_POWER * (jnp.maximum(u, 0.0) + jnp.log1p(jnp.exp(-jnp.abs(u))))
+    for i in range(2):
         halo_copy(i).wait()
     first = s == 0
     xpad[pl.ds(0, 8)] = halo[...].astype(F32)[8:16]
-    idpad[pl.ds(0, 8)] = jnp.where(first, -1, ihalo[...])
-
-    def fill(i, _):
-        r = pl.multiple_of(i * CH, CH)
-        xpad[pl.ds(pl.multiple_of(r + 8, 8), CH)] = recur[pl.ds(r, CH)].astype(F32)
-        idpad[pl.ds(pl.multiple_of(r + 8, 8), CH)] = ids[pl.ds(r, CH)]
-        return 0
-
-    lax.fori_loop(0, tok // CH, fill, 0)
-
+    idpad[pl.ds(0, 8)] = jnp.where(first, -1, down_rows(ihalo[tok // 128 - 1:tok // 128])[120:])
     reps = loc // 128
     ntaps = taps.shape[0]
 
@@ -683,7 +700,7 @@
         xw = xpad[pl.ds(r, CH + 8)]
         iw = idpad[pl.ds(r, CH + 8)]
         mine = iw[8:]
-        tw = taps[...]
+        tw = taps[...].astype(F32)
         conv = xw[8:] * tw[0:1]
         cont = None
         for k in range(1, ntaps):
@@ -695,7 +712,7 @@
         cb = conv.astype(BF16)
         rg = jax.nn.sigmoid(jnp.dot(cb, bd[0], preferred_element_type=F32))
         ig = jax.nn.sigmoid(jnp.dot(cb, bd[1], preferred_element_type=F32))
-        ld = rate[...] * rg + extra[pl.ds(r, CH)]
+        ld = rate * rg + extra[pl.ds(r, CH)]
         fac[pl.ds(r, CH)] = jnp.exp(ld) * cont
         drv[pl.ds(r, CH)] = jnp.sqrt(one_minus_exp(2.0 * ld)) * ig * cb.astype(F32)
         return 0
@@ -705,10 +722,6 @@
     @pl.when(y == core)
     def _():
         load_seed(UP[0])
-
-    @pl.when(y != core)
-    def _():
-        push_seed(GATE[0])
 
     rows8 = lax.broadcasted_iota(jnp.int32, (8, loc), 0)
 
@@ -745,8 +758,9 @@
 
     @pl.when(y != core)
     def _():
+        for a in GATE:
+            push_seed(a)
         load_seed(UP[0])
-        push_seed(GATE[1])
 
     for a in DOWN:
         load_seed(a)
@@ -765,6 +779,9 @@
         carry = jnp.where(o < s, e[:8] * carry + e[8:], carry)
     cin = carry[0:1]
 
+    for i in range(2, len(inputs)):
+        load_input(i).wait()
+
     def branch(i, _):
         r = pl.multiple_of(i * CH, CH)
         st = drv[pl.ds(r, CH)] + fac[pl.ds(r, CH)] * cin
@@ -841,7 +858,7 @@
             ssq[q, t, :, pl.ds(r, BR)] = jnp.transpose(jnp.broadcast_to(c, (BR, 128)))[:8]
             return 0
 
-        lax.fori_loop(0, tok // BR, write, 0)
+        lax.fori_loop(0, tok // BR, write, 0, unroll=True)
         for j in range(1, ntp):
             tp_push(lambda o: ssq.at[q, o], qsend.at[q], qrecv.at[q], j, True).start()
 
@@ -880,7 +897,7 @@
         mixed[pl.ds(r, BR)] = (residual[pl.ds(r, BR)].astype(F32) + m * inverse_rms(0, r) * mix_gain[...]).astype(BF16)
         return 0
 
-    lax.fori_loop(0, tok // BR, stream, 0)
+    lax.fori_loop(0, tok // BR, stream, 0, unroll=True)
     row_total(1, lambda r: mixed[pl.ds(r, BR)].astype(F32))
     wait_total(1)
 
@@ -898,7 +915,7 @@
 
         return 0
 
-    lax.fori_loop(0, tok // BR, norm, 0)
+    lax.fori_loop(0, tok // BR, norm, 0, unroll=True)
 
     def n_copy(dy, dx):
         return pltpu.make_async_remote_copy(
@@ -1101,26 +1118,29 @@
     def _():
         p_wait(0, 0)
 
-    def gather_sum(i, _):
-        r = pl.multiple_of(i * BR, BR)
+    def ffn_rows(r):
         for w in range(per):
             total = recvd[0, w, pl.ds(r, BR)].astype(F32)
             for k in range(1, ny * chips):
                 total = total + recvd[k, w, pl.ds(r, BR)].astype(F32)
             out[pl.ds(r, BR), pl.ds(w * ncol, ncol)] = total.astype(BF16)
-        return 0
-
-    lax.fori_loop(0, tok // BR, gather_sum, 0)
-    row_total(2, lambda r: out[pl.ds(r, BR)].astype(F32))
+        return out[pl.ds(r, BR)].astype(F32)
+
+    row_total(2, ffn_rows)
     wait_total(2)
+
+    def out_copy(i):
+        rows = pl.ds(pl.multiple_of(i * BR, BR), BR)
+        return pltpu.make_async_copy(out.at[rows], out_hbm.at[rows], osem.at[i])
 
     def finish(i, _):
         r = pl.multiple_of(i * BR, BR)
         f = out[pl.ds(r, BR)].astype(F32)
         out[pl.ds(r, BR)] = (mixed[pl.ds(r, BR)].astype(F32) + f * inverse_rms(2, r) * ffn_gain[...]).astype(BF16)
-        return 0
-
-    lax.fori_loop(0, tok // BR, finish, 0)
+        out_copy(i).start()
+        return 0
+
+    lax.fori_loop(0, tok // BR, finish, 0, unroll=True)
 
     def sent(c):
         c.wait_send()
@@ -1144,6 +1164,8 @@
     for j in range(1, ntp):
         for q in range(3):
             tp_push(lambda o: ssq.at[q, o], qsend.at[q], qrecv.at[q], j, True).wait_send()
+    for i in range(tok // BR):
+        out_copy(i).wait()
 
 
 def body(n, ntp, gate_branch, recur_input, doc_ids, conv_taps, gate_map, input_map, decay_level, decay_extra,
@@ -1154,9 +1176,14 @@
     ncol = down_weight.shape[1]
     heads, head, _ = gate_map.shape
     nz, ny = grid_of(n)
-    ids = jnp.broadcast_to(doc_ids[:, None], (tok, 128))
-    rate = (GATE_POWER * -jax.nn.softplus(-decay_level))[None, :]
-    args = (gate_branch, recur_input, ids, conv_taps.astype(F32), gate_map.reshape(heads * head, head),
+    planes = ny == 2 and tok % 128 == 0
+    if planes:
+        ids, taps, rate = doc_ids.reshape(tok // 128, 128), conv_taps, decay_level[None, :]
+    else:
+        ids = jnp.broadcast_to(doc_ids[:, None], (tok, 128))
+        taps = conv_taps.astype(F32)
+        rate = (GATE_POWER * -jax.nn.softplus(-decay_level))[None, :]
+    args = (gate_branch, recur_input, ids, taps, gate_map.reshape(heads * head, head),
             input_map.reshape(heads * head, head), rate, decay_extra, out_weight, residual,
             mix_gain[None, :], pre_gain[None, :], ffn_gain[None, :], gate_weight, up_weight, down_weight)
     vm = pl.BlockSpec(memory_space=pltpu.VMEM)
@@ -1164,11 +1191,15 @@
     V, S = pltpu.VMEM, pltpu.SemaphoreType.DMA
     per = dloc // ncol
     chips = ntp // 2
-    if ny == 2:
+    if planes:
         fn = plane_kernel
+        in_specs = [hbm] * 2 + [vm] * 5 + [hbm] * 3 + [vm] * 3 + [hbm] * 3
+        out_spec = hbm
         scratch = [
+            V((tok, dloc), BF16), S((tok // math.gcd(tok, 128),)),
+            V((tok, loc), BF16), V((tok, loc), BF16), V((tok, loc), F32), V(out_weight.shape, BF16), V((tok, dloc), BF16), S((5,)),
             V((n * krows, ff), BF16), V((n * krows, ff), BF16), V((n, ff, ncol), BF16),
-            V((tok + 8, loc), F32), V((tok + 8, 128), jnp.int32), V((16, loc), BF16), V((8, 128), jnp.int32),
+            V((tok + 8, loc), F32), V((tok + 8, 128), jnp.int32), V((16, loc), BF16), V((tok // 128, 128), jnp.int32),
             V((2, loc, loc), BF16), V((tok, loc), F32), V((tok, loc), F32), V((n, 16, loc), F32),
             V((ntp, tok, loc), BF16), V((tok, dloc), BF16), V((tok, dloc), BF16), V((tok, dloc * ntp), BF16),
             V((tok, ff), F32), V((tok, ff), F32), V((tok, ff), BF16), V((n, tok, ncol), BF16), V((ny * chips, per, tok, ncol), BF16), V((3, ntp, 8, tok), F32),
@@ -1178,6 +1209,8 @@
         ]
     else:
         fn = kernel
+        in_specs = [vm] * 13 + [hbm] * 3
+        out_spec = vm
         scratch = [
             V((n * krows, ff), BF16), V((n * krows, ff), BF16), V((n, ff, ncol), BF16),
             V((tok + 8, loc), F32), V((tok + 8, 128), jnp.int32), V((16, loc), BF16), V((8, 128), jnp.int32),
@@ -1192,8 +1225,8 @@
     return pl.pallas_call(
         functools.partial(fn, (n, ntp, nz, ny, dloc * ntp)),
         out_shape=jax.ShapeDtypeStruct((tok, dloc), BF16),
-        in_specs=[vm] * 13 + [hbm] * 3,
-        out_specs=vm,
+        in_specs=in_specs,
+        out_specs=out_spec,
         scratch_shapes=scratch,
         compiler_params=pltpu.CompilerParams(
             collective_id=0, has_side_effects=True, vmem_limit_bytes=62 * 1024 * 1024),

time: 181 us -> 176 us (0.972)
  Pallas kernels: 176 us -> 174 us
    pallas_call x1, Pallas kernels: 176 us -> 174 us  [body(): pl.pallas_call(functools.partial(fn, (n, ntp, nz, ny, dloc * ntp)), out_s...]
where the time goes in v3:
time: 176 us
  Pallas kernels  174 us (99%)
  local copies, waits for them, and re-layouts  2.06 us (1%)
    pallas_call x1, Pallas kernels, body(): pl.pallas_call(functools.partial(fn, (n, ntp, nz, ny, dloc * ntp)), out_s...  174 us

profile of v3, /device:TPU:5, one launch (start us, length us, event | category | flops | bytes accessed | tf_op | source)
XLA Modules:
  0.0 176.3 jit_solution(517499318395424417)
XLA Ops:
  0.0 174.2 %shard_map.154 = bf16[768,512]{1,0:T(8,128)(2,1)} custom-call(bf16[768,256]{1,0:T(8,128)(2,1)} %gate_branch_in.1, bf16[768,256]{1,0:T(8,128)(2,1)} %recur_in.1, s32[6,128]{1,0:T(8,128)} %bitcast.9, bf16[4,256]{1,0:T(4,128)(2,1)} %taps.1, bf16[256,64]{1,0:T(8,128)(2,1)} %bitcast.7, bf16[256,64]{1,0:T(8,128)(2,1)} %bitcast.8, f32[1,256]{1,0:T(1,128)} %bitcast.13, ...), custom_call_target="tpu_custom_call" | custom-call | tf_op jit(solution)/shard_map/pallas_call | solution.py:1225
  174.2 2.1 %copy.18 = bf16[768,512]{1,0:T(8,128)(2,1)} copy(bf16[768,512]{1,0:T(8,128)(2,1)} %shard_map.154) | data formatting | bytes 1572864

commit v4 on v3

--- a/solution.py
+++ b/solution.py
@@ -507,9 +507,9 @@
     out_hbm,
     out, osem, gate_branch, recur, extra, out_w, residual, insem,
     gate_all, up_all, down_all, xpad, idpad, halo, ihalo, bd, fac, drv, ends, bfull,
-    mixed, nloc, normed, gsum, usum, hidden, partial, recvd, ssq,
+    mixed, nloc, gloc, normed, gnormed, ghid, gsum, usum, hidden, partial, recvd, ssq,
     lsem, ssend, srecv, zsend, zrecv, msend, mrecv,
-    hsend, hrecv, esend, erecv, bsend, brecv, nsend, nrecv, qsend, qrecv, psend, precv,
+    hsend, hrecv, esend, erecv, bsend, brecv, nsend, nrecv, fsend, frecv, gsend, grecv, qsend, qrecv, psend, precv,
 ):
     n, ntp, nz, ny, width = cfg
     s, t = lax.axis_index("sp"), lax.axis_index("tp")
@@ -557,21 +557,31 @@
 
     hcol = ncol // 2
     hrow = krows // 2
-    GATE, UP, DOWN = (0, 1), (2,), (3, 4)
+    GATE, UP, DOWN, WIDE = (0, 1), (2,), (3, 4), (5, 6)
+    fa = ff - ghid.shape[1]
+    main, side = pl.ds(0, fa), pl.ds(fa, ff - fa)
+    inner = jnp.logical_and(z > 0, z < nz - 1)
+    host = jnp.logical_or(z == 1, z == nz - 2)
+    guest_z = jnp.where(z == 1, 0, nz - 1)
+    host_z = jnp.where(z == 0, 1, nz - 2)
 
     def block(a, o, b):
         i = o * ny + b
         if a in GATE:
-            return gate_all.at[pl.ds(pl.multiple_of(i * krows + a * hrow, hrow), hrow)]
+            return gate_all.at[pl.ds(pl.multiple_of(i * krows + a * hrow, hrow), hrow), main]
         if a in UP:
-            return up_all.at[pl.ds(pl.multiple_of(i * krows, krows), krows)]
+            return up_all.at[pl.ds(pl.multiple_of(i * krows, krows), krows), main]
+        if a in WIDE:
+            return (gate_all, up_all)[a - WIDE[0]].at[pl.ds(pl.multiple_of(i * krows, krows), krows), side]
         return down_all.at[i, :, pl.ds((a - DOWN[0]) * hcol, hcol)]
 
     def own_shard(a):
         if a in GATE:
-            return gate_w.at[pl.ds(a * hrow, hrow)]
+            return gate_w.at[pl.ds(a * hrow, hrow), main]
         if a in UP:
-            return up_w
+            return up_w.at[:, main]
+        if a in WIDE:
+            return (gate_w, up_w)[a - WIDE[0]].at[:, side]
         return down_w.at[:, pl.ds((a - DOWN[0]) * hcol, hcol)]
 
     def seed_local(a):
@@ -595,19 +605,24 @@
             device_id=(s, mate), device_id_type=MESH)
 
     def fan_down(a, o, act):
-        @pl.when(jnp.logical_and(o >= z, z > 0))
+        @pl.when(jnp.logical_and(o >= z, z > (1 if a in WIDE else 0)))
         def _():
             act(z_copy(a, o, 0))
 
     def fan_up(a, o, act):
-        @pl.when(jnp.logical_and(o <= z, z < nz - 1))
+        @pl.when(jnp.logical_and(o <= z, z < nz - (2 if a in WIDE else 1)))
         def _():
             act(z_copy(a, o, 1))
 
     def fan(a, o, act):
         fan_down(a, o, act)
         fan_up(a, o, act)
-        act(mate_copy(a, o))
+        if a in WIDE:
+            @pl.when(inner)
+            def _():
+                act(mate_copy(a, o))
+        else:
+            act(mate_copy(a, o))
 
     def start(c):
         c.start()
@@ -721,7 +736,8 @@
 
     @pl.when(y == core)
     def _():
-        load_seed(UP[0])
+        for a in UP + WIDE:
+            load_seed(a)
 
     rows8 = lax.broadcasted_iota(jnp.int32, (8, loc), 0)
 
@@ -760,16 +776,17 @@
     def _():
         for a in GATE:
             push_seed(a)
-        load_seed(UP[0])
+        for a in UP + WIDE:
+            load_seed(a)
 
     for a in DOWN:
         load_seed(a)
 
     @pl.when(y == core)
     def _():
-        push_seed(UP[0])
-
-    inner = jnp.logical_and(z > 0, z < nz - 1)
+        for a in UP + WIDE:
+            push_seed(a)
+
     early = min(2, nz - 1)
     for j in range(1, n):
         end_arrived(j)
@@ -840,12 +857,8 @@
 
     @pl.when(y != core)
     def _():
-        push_seed(UP[0])
-
-    @pl.when(inner)
-    def _():
-        for j in range(1, early + 1):
-            relay(GATE, j)
+        for a in UP + WIDE:
+            push_seed(a)
 
     gather_share(bview, bsend, brecv)
     gather_wait(bview, bsend, brecv)
@@ -887,7 +900,7 @@
     @pl.when(inner)
     def _():
         for j in range(1, early + 1):
-            relay(UP, j)
+            relay(GATE, j)
 
     wait_total(0)
 
@@ -916,41 +929,109 @@
         return 0
 
     lax.fori_loop(0, tok // BR, norm, 0, unroll=True)
-
-    def n_copy(dy, dx):
-        return pltpu.make_async_remote_copy(
-            src_ref=nloc, dst_ref=normed.at[:, cols], send_sem=nsend.at[dy, dx], recv_sem=nrecv.at[t],
+    htok = tok // 2
+    piece, spot = (nloc, gloc), (normed, gnormed)
+
+    def n_copy(q, dy, dx):
+        return pltpu.make_async_remote_copy(
+            src_ref=piece[q], dst_ref=spot[q].at[:, cols], send_sem=nsend.at[q, dy, dx], recv_sem=nrecv.at[q, t],
             device_id=(z * ny + lax.rem(y + dy, ny), 2 * lax.rem(x + dx, chips) + y), device_id_type=MESH)
 
-    def to_plane(act):
-        for dy in range(ny):
-            for dx in range(chips):
-                if dy or dx:
-                    act(n_copy(dy, dx))
-                else:
-                    @pl.when(y != core)
-                    def _():
-                        act(n_copy(0, 0))
-
-    def n_wait(dt):
-        o = lax.rem(t + dt, ntp)
-        view = normed.at[:, pl.ds(pl.multiple_of(o * dloc, dloc), dloc)]
+    def to_plane(q, act):
+        for dx in range(1, chips):
+            act(n_copy(q, 0, dx))
+        for dy in range(1, ny):
+            act(n_copy(q, dy, 0))
+
+        @pl.when(y != core)
+        def _():
+            act(n_copy(q, 0, 0))
+
+    def n_wait(q, o):
+        view = spot[q].at[:, pl.ds(pl.multiple_of(o * dloc, dloc), dloc)]
         pltpu.make_async_remote_copy(
-            src_ref=view, dst_ref=view, send_sem=nsend.at[0, 0], recv_sem=nrecv.at[o],
+            src_ref=view, dst_ref=view, send_sem=nsend.at[q, 0, 0], recv_sem=nrecv.at[q, o],
             device_id=(s, mate), device_id_type=MESH).wait_recv()
 
-    to_plane(start)
+    def f_copy(q, o, h, device):
+        view = spot[q].at[pl.ds(h * htok, htok), pl.ds(pl.multiple_of(o * dloc, dloc), dloc)]
+        return pltpu.make_async_remote_copy(
+            src_ref=view, dst_ref=view, send_sem=fsend.at[q, lax.rem(o, 2)], recv_sem=frecv.at[q, h, o],
+            device_id=device, device_id_type=MESH)
+
+    other = 1 - x
+
+    def forward(q, act, wait):
+        for e in range(2):
+            @pl.when(y == core)
+            def _():
+                o = 2 * other + e
+                if wait:
+                    n_wait(q, o)
+                act(f_copy(q, o, 0, (z * ny + 1 - y, t)))
+
+            @pl.when(y != core)
+            def _():
+                o = 2 * x + e
+                if wait:
+                    n_wait(q, o)
+                act(f_copy(q, o, 1, (s, 2 * other + core)))
+
+    def n_ready(q):
+        @pl.when(y == core)
+        def _():
+            n_wait(q, mate)
+
+        @pl.when(y != core)
+        def _():
+            for e in range(2):
+                for h in range(2):
+                    f_copy(q, 2 * other + e, h, (s, mate)).wait_recv()
+
+    def guest_hop():
+        return pltpu.make_async_remote_copy(
+            src_ref=nloc, dst_ref=gloc, send_sem=gsend.at[0], recv_sem=grecv.at[0],
+            device_id=(host_z * ny + y, t), device_id_type=MESH)
+
+    def guest_return():
+        return pltpu.make_async_remote_copy(
+            src_ref=ghid, dst_ref=hidden.at[:, side], send_sem=gsend.at[1], recv_sem=grecv.at[1],
+            device_id=(guest_z * ny + y, t), device_id_type=MESH)
+
+    to_plane(0, start)
 
     @pl.when(jnp.logical_not(inner))
     def _():
+        guest_hop().start()
         for a in DOWN:
             push_seed(a)
+
+    @pl.when(inner)
+    def _():
+        for j in range(1, early + 1):
+            relay(UP, j)
+            relay(WIDE, j)
+
+    forward(0, start, True)
+
+    @pl.when(host)
+    def _():
+        guest_hop().wait_recv()
+
+        @pl.when(y == core)
+        def _():
+            gnormed[:, cols] = gloc[...]
+
+        to_plane(1, start)
+
+    @pl.when(jnp.logical_not(inner))
+    def _():
         for j in range(1, early + 1):
             relay(GATE, j)
             relay(UP, j)
 
-    def outward_seed():
-        for a in DOWN:
+    def outward_seed(items):
+        for a in items:
             @pl.when(low == 1)
             def _():
                 fan_down(a, z, start)
@@ -959,23 +1040,13 @@
             def _():
                 fan_up(a, z, start)
 
-    def mates(js):
+    def mates(items, js):
         for j in js:
-            for a in GATE + UP:
+            for a in items:
                 mate_copy(a, origin[j], True).wait_recv()
-
-    def n_ready():
-        for dt in range(1, ntp):
-            n_wait(dt)
-
-        @pl.when(y != core)
-        def _():
-            n_wait(0)
 
     kblk = ny * krows
     TN = 256
-    tiles = ff // TN
-
     def sums(js, cs):
         g = u = None
         for j in js:
@@ -1001,15 +1072,20 @@
             tile(pl.multiple_of(j * TN, TN), TN)
             return 0
 
-        lax.fori_loop(0, tiles, step, 0)
-        if ff % TN:
-            tile(tiles * TN, ff % TN)
+        lax.fori_loop(0, fa // TN, step, 0)
+        if fa % TN:
+            tile(fa // TN * TN, fa % TN)
+
+        @pl.when(inner)
+        def _():
+            tile(fa, ff - fa)
 
     @pl.when(inner)
     def _():
         for j in range(early + 1, nz):
             relay(GATE, j)
             relay(UP, j)
+            relay(WIDE, j)
         for a in DOWN:
             seed_ready(a)
             mate_copy(a, z).start()
@@ -1022,13 +1098,21 @@
             def _():
                 fan_down(a, z, start)
 
-        @pl.when(core == 0)
-        def _():
-            outward_seed()
-
-    n_ready()
-    mates(range(nz - 1))
+        outward_seed(DOWN[:1])
+        relay(DOWN, 2)
+
+    n_ready(0)
+    mates(GATE + UP, range(nz - 1))
+
+    @pl.when(inner)
+    def _():
+        mates(WIDE, range(nz - 1))
+
     over_tiles(first_tile)
+
+    @pl.when(host)
+    def _():
+        forward(1, start, True)
 
     @pl.when(jnp.logical_not(inner))
     def _():
@@ -1036,8 +1120,25 @@
             relay(GATE, j)
             relay(UP, j)
 
-    mates((nz - 1,))
+    mates(GATE + UP, (nz - 1,))
+
+    @pl.when(inner)
+    def _():
+        mates(WIDE, (nz - 1,))
+
     over_tiles(last_tile)
+
+    @pl.when(host)
+    def _():
+        n_ready(1)
+        g = jnp.dot(gnormed[...], gate_all[:, side], preferred_element_type=F32)
+        v = jnp.dot(gnormed[...], up_all[:, side], preferred_element_type=F32)
+        ghid[...] = (jax.nn.silu(g) * v).astype(BF16)
+        guest_return().start()
+
+    @pl.when(jnp.logical_not(inner))
+    def _():
+        guest_return().wait_recv()
 
     me = y * chips + x
 
@@ -1069,16 +1170,27 @@
             mate_copy(a, o, True).wait_recv()
 
     def order(b, j):
-        if b == 0 or j == 0:
+        if j == 0:
             return origin[j]
-        return jnp.where(inner, origin[j], origin[1 + j % (nz - 1)])
+        line = origin[2:3] + (origin[1:2] + origin[3:] if b == 0 else origin[3:] + origin[1:2])
+        return jnp.where(inner, origin[j], line[j - 1])
 
     for j in range(nz):
         mine = jnp.where(core == 0, order(0, j), order(1, j))
         if j < nz - 1:
-            if j:
+            if j == 2:
+                @pl.when(jnp.logical_not(inner))
+                def _():
+                    for a in DOWN:
+                        relay_from(a, mine)
+            elif j:
                 for a in DOWN:
                     relay_from(a, mine)
+            if j == 1:
+                @pl.when(jnp.logical_and(inner, core == 0))
+                def _():
+                    outward_seed(DOWN[1:])
+
             for b in range(ny):
                 i = order(b, j) * ny + b
                 for a in DOWN:
@@ -1091,7 +1203,7 @@
                 if h == 1:
                     @pl.when(jnp.logical_and(inner, core == 1))
                     def _():
-                        outward_seed()
+                        outward_seed(DOWN[1:])
 
                 c = pl.ds(h * hcol, hcol)
                 for b in range(ny):
@@ -1145,7 +1257,7 @@
     def sent(c):
         c.wait_send()
 
-    for a in GATE + UP + DOWN:
+    for a in GATE + UP + DOWN + WIDE:
         @pl.when(y != core)
         def _():
             seed_swap(a).wait_send()
@@ -1155,7 +1267,19 @@
     for j in range(1, n):
         end_copy(j).wait_send()
     gather_sent(bview, bsend, brecv)
-    to_plane(sent)
+    to_plane(0, sent)
+    forward(0, sent, False)
+
+    @pl.when(host)
+    def _():
+        to_plane(1, sent)
+        forward(1, sent, False)
+        guest_return().wait_send()
+
+    @pl.when(jnp.logical_not(inner))
+    def _():
+        guest_hop().wait_send()
+
     for i in range(n):
         @pl.when(jnp.logical_not(owned(i)))
         def _():
@@ -1176,7 +1300,8 @@
     ncol = down_weight.shape[1]
     heads, head, _ = gate_map.shape
     nz, ny = grid_of(n)
-    planes = ny == 2 and tok % 128 == 0
+    planes = ny == 2 and nz > 3 and ntp == 4 and tok % 256 == 0 and ff % 128 == 0
+    fb = ff // 128 * 2 // 11 * 128
     if planes:
         ids, taps, rate = doc_ids.reshape(tok // 128, 128), conv_taps, decay_level[None, :]
     else:
@@ -1201,11 +1326,11 @@
             V((n * krows, ff), BF16), V((n * krows, ff), BF16), V((n, ff, ncol), BF16),
             V((tok + 8, loc), F32), V((tok + 8, 128), jnp.int32), V((16, loc), BF16), V((tok // 128, 128), jnp.int32),
             V((2, loc, loc), BF16), V((tok, loc), F32), V((tok, loc), F32), V((n, 16, loc), F32),
-            V((ntp, tok, loc), BF16), V((tok, dloc), BF16), V((tok, dloc), BF16), V((tok, dloc * ntp), BF16),
-            V((tok, ff), F32), V((tok, ff), F32), V((tok, ff), BF16), V((n, tok, ncol), BF16), V((ny * chips, per, tok, ncol), BF16), V((3, ntp, 8, tok), F32),
-            S((5,)), S((5,)), S((5,)), S((2, 5, nz)), S((5, nz)), S((5, nz)), S((5, nz)),
+            V((ntp, tok, loc), BF16), V((tok, dloc), BF16), V((tok, dloc), BF16), V((tok, dloc), BF16), V((tok, dloc * ntp), BF16),
+            V((tok, dloc * ntp), BF16), V((tok, fb), BF16), V((tok, ff), F32), V((tok, ff), F32), V((tok, ff), BF16), V((n, tok, ncol), BF16), V((ny * chips, per, tok, ncol), BF16), V((3, ntp, 8, tok), F32),
+            S((7,)), S((7,)), S((7,)), S((2, 7, nz)), S((7, nz)), S((7, nz)), S((7, nz)),
             S((2,)), S((2,)), S((n - 1,)), S((n - 1,)), S((ntp - 1,)), S((ntp - 1,)),
-            S((ny, chips)), S((ntp,)), S((3, ntp - 1)), S((3, ntp - 1)), S((n, 2)), S((ny * chips, per, 2)),
+            S((2, ny, chips)), S((2, ntp)), S((2, 2)), S((2, 2, ntp)), S((2,)), S((2,)), S((3, ntp - 1)), S((3, ntp - 1)), S((n, 2)), S((ny * chips, per, 2)),
         ]
     else:
         fn = kernel

time: 176 us -> 169 us (0.960)
  the two profiles are of different devices: /device:TPU:5 before, /device:TPU:0 now
where the time goes in v4:
time: 169 us
  Pallas kernels  167 us (99%)
  local copies, waits for them, and re-layouts  2.06 us (1%)
    pallas_call x1, Pallas kernels, body(): pl.pallas_call(functools.partial(fn, (n, ntp, nz, ny, dloc * ntp)), out_s...  167 us

profile of v4, /device:TPU:0, one launch (start us, length us, event | category | flops | bytes accessed | tf_op | source)
XLA Modules:
  0.0 169.2 jit_solution(3256703810223931119)
XLA Ops:
  0.0 167.2 %shard_map.154 = bf16[768,512]{1,0:T(8,128)(2,1)} custom-call(bf16[768,256]{1,0:T(8,128)(2,1)} %gate_branch_in.1, bf16[768,256]{1,0:T(8,128)(2,1)} %recur_in.1, s32[6,128]{1,0:T(8,128)} %bitcast.9, bf16[4,256]{1,0:T(4,128)(2,1)} %taps.1, bf16[256,64]{1,0:T(8,128)(2,1)} %bitcast.7, bf16[256,64]{1,0:T(8,128)(2,1)} %bitcast.8, f32[1,256]{1,0:T(1,128)} %bitcast.13, ...), custom_call_target="tpu_custom_call" | custom-call | tf_op jit(solution)/shard_map/pallas_call | solution.py:1350
  167.2 2.1 %copy.18 = bf16[768,512]{1,0:T(8,128)(2,1)} copy(bf16[768,512]{1,0:T(8,128)(2,1)} %shard_map.154) | data formatting | bytes 1572864

commit v5 on v4

--- a/solution.py
+++ b/solution.py
@@ -1169,48 +1169,57 @@
         def _():
             mate_copy(a, o, True).wait_recv()
 
-    def order(b, j):
-        if j == 0:
-            return origin[j]
-        line = origin[2:3] + (origin[1:2] + origin[3:] if b == 0 else origin[3:] + origin[1:2])
-        return jnp.where(inner, origin[j], line[j - 1])
-
-    for j in range(nz):
-        mine = jnp.where(core == 0, order(0, j), order(1, j))
-        if j < nz - 1:
-            if j == 2:
-                @pl.when(jnp.logical_not(inner))
-                def _():
-                    for a in DOWN:
-                        relay_from(a, mine)
-            elif j:
-                for a in DOWN:
-                    relay_from(a, mine)
-            if j == 1:
-                @pl.when(jnp.logical_and(inner, core == 0))
-                def _():
-                    outward_seed(DOWN[1:])
-
-            for b in range(ny):
-                i = order(b, j) * ny + b
-                for a in DOWN:
-                    mate_ready(a, order(b, j), b)
-                partial[i] = jnp.dot(hidden[...], down_all[i], preferred_element_type=F32).astype(BF16)
-                ship(i, (0, 1))
-        else:
-            for h in range(2):
-                relay_from(DOWN[h], mine)
-                if h == 1:
-                    @pl.when(jnp.logical_and(inner, core == 1))
-                    def _():
-                        outward_seed(DOWN[1:])
-
-                c = pl.ds(h * hcol, hcol)
-                for b in range(ny):
-                    i = order(b, j) * ny + b
-                    mate_ready(DOWN[h], order(b, j), b)
-                    partial[i, :, c] = jnp.dot(hidden[...], down_all[i, :, c], preferred_element_type=F32).astype(BF16)
-                    ship(i, (h,))
+    last = nz - 1
+    ends_order = [0] + list(range(2, nz)) + [1]
+    line = [jnp.where(inner, origin[j], origin[ends_order[j]]) for j in range(nz)]
+    roles = (y, 1 - y)
+
+    def bring(j, k, items):
+        @pl.when(jnp.logical_and(roles[k] == core, jnp.logical_not(inner) if j == 2 else True))
+        def _():
+            for a in items:
+                relay_from(a, line[j])
+
+    def whole_block(j, k):
+        i = line[j] * ny + roles[k]
+        if j:
+            bring(j, k, DOWN)
+        for a in DOWN:
+            mate_ready(a, line[j], roles[k])
+        partial[i] = jnp.dot(hidden[...], down_all[i], preferred_element_type=F32).astype(BF16)
+        ship(i, (0, 1))
+
+    def half_block(j, k, h):
+        i = line[j] * ny + roles[k]
+        c = pl.ds(h * hcol, hcol)
+        mate_ready(DOWN[h], line[j], roles[k])
+        partial[i, :, c] = jnp.dot(hidden[...], down_all[i, :, c], preferred_element_type=F32).astype(BF16)
+        ship(i, (h,))
+
+    def outward_rest(k):
+        @pl.when(jnp.logical_and(inner, roles[k] == core))
+        def _():
+            outward_seed(DOWN[1:])
+
+    for j in range(2):
+        for k in range(2):
+            whole_block(j, k)
+    for k in range(2):
+        bring(last, k, DOWN[:1])
+        half_block(last, k, 0)
+    for j in range(2, last):
+        whole_block(j, 0)
+    for j in range(2, last):
+        for h in range(2):
+            if j == last - 1 and h == 1:
+                bring(last, 0, DOWN[1:])
+                outward_rest(0)
+            bring(j, 1, DOWN[h:h + 1])
+            half_block(j, 1, h)
+    bring(last, 1, DOWN[1:])
+    outward_rest(1)
+    for k in range(2):
+        half_block(last, k, 1)
 
     def p_wait(dy, dx):
         k = lax.rem(y + dy, ny) * chips + lax.rem(x + dx, chips)

time: 169 us -> 165 us (0.976)
  Pallas kernels: 167 us -> 162 us
    pallas_call x1, Pallas kernels: 167 us -> 162 us  [body(): pl.pallas_call(functools.partial(fn, (n, ntp, nz, ny, dloc * ntp)), out_s...]
where the time goes in v5:
time: 165 us; the launch traced here: 164 us
  Pallas kernels  162 us (98%)
  local copies, waits for them, and re-layouts  2.06 us (1%)
    pallas_call x1, Pallas kernels, body(): pl.pallas_call(functools.partial(fn, (n, ntp, nz, ny, dloc * ntp)), out_s...  162 us

profile of v5, /device:TPU:0, one launch (start us, length us, event | category | flops | bytes accessed | tf_op | source)
XLA Modules:
  0.0 164.5 jit_solution(4709246880699780547)
XLA Ops:
  0.0 162.4 %shard_map.154 = bf16[768,512]{1,0:T(8,128)(2,1)} custom-call(bf16[768,256]{1,0:T(8,128)(2,1)} %gate_branch_in.1, bf16[768,256]{1,0:T(8,128)(2,1)} %recur_in.1, s32[6,128]{1,0:T(8,128)} %bitcast.9, bf16[4,256]{1,0:T(4,128)(2,1)} %taps.1, bf16[256,64]{1,0:T(8,128)(2,1)} %bitcast.7, bf16[256,64]{1,0:T(8,128)(2,1)} %bitcast.8, f32[1,256]{1,0:T(1,128)} %bitcast.13, ...), custom_call_target="tpu_custom_call" | custom-call | tf_op jit(solution)/shard_map/pallas_call | solution.py:1359
  162.4 2.1 %copy.18 = bf16[768,512]{1,0:T(8,128)(2,1)} copy(bf16[768,512]{1,0:T(8,128)(2,1)} %shard_map.154) | data formatting | bytes 1572864

commit v6 on v5

--- a/solution.py
+++ b/solution.py
@@ -1182,8 +1182,6 @@
 
     def whole_block(j, k):
         i = line[j] * ny + roles[k]
-        if j:
-            bring(j, k, DOWN)
         for a in DOWN:
             mate_ready(a, line[j], roles[k])
         partial[i] = jnp.dot(hidden[...], down_all[i], preferred_element_type=F32).astype(BF16)
@@ -1201,21 +1199,36 @@
         def _():
             outward_seed(DOWN[1:])
 
-    for j in range(2):
+    @pl.when(jnp.logical_not(inner))
+    def _():
         for k in range(2):
-            whole_block(j, k)
+            bring(last, k, DOWN[:1])
+
     for k in range(2):
-        bring(last, k, DOWN[:1])
+        whole_block(0, k)
+    bring(1, 0, DOWN)
+    whole_block(1, 0)
+    bring(1, 1, DOWN)
+    whole_block(1, 1)
+
+    @pl.when(inner)
+    def _():
+        for k in range(2):
+            bring(last, k, DOWN[:1])
+
+    for k in range(2):
         half_block(last, k, 0)
     for j in range(2, last):
+        bring(j, 0, DOWN)
+        bring(j, 1, DOWN[:1])
         whole_block(j, 0)
     for j in range(2, last):
-        for h in range(2):
-            if j == last - 1 and h == 1:
-                bring(last, 0, DOWN[1:])
-                outward_rest(0)
-            bring(j, 1, DOWN[h:h + 1])
-            half_block(j, 1, h)
+        half_block(j, 1, 0)
+        if j == last - 1:
+            bring(last, 0, DOWN[1:])
+            outward_rest(0)
+        bring(j, 1, DOWN[1:])
+        half_block(j, 1, 1)
     bring(last, 1, DOWN[1:])
     outward_rest(1)
     for k in range(2):

time: 165 us -> 163 us (0.988)
    pallas_call x1, Pallas kernels: 162 us -> 161 us  [body(): pl.pallas_call(functools.partial(fn, (n, ntp, nz, ny, dloc * ntp)), out_s...]
where the time goes in v6:
time: 163 us
  Pallas kernels  161 us (99%)
  local copies, waits for them, and re-layouts  2.06 us (1%)
    pallas_call x1, Pallas kernels, body(): pl.pallas_call(functools.partial(fn, (n, ntp, nz, ny, dloc * ntp)), out_s...  161 us

profile of v6, /device:TPU:0, one launch (start us, length us, event | category | flops | bytes accessed | tf_op | source)
XLA Modules:
  0.0 162.8 jit_solution(1794664938477785615)
XLA Ops:
  0.0 160.7 %shard_map.154 = bf16[768,512]{1,0:T(8,128)(2,1)} custom-call(bf16[768,256]{1,0:T(8,128)(2,1)} %gate_branch_in.1, bf16[768,256]{1,0:T(8,128)(2,1)} %recur_in.1, s32[6,128]{1,0:T(8,128)} %bitcast.9, bf16[4,256]{1,0:T(4,128)(2,1)} %taps.1, bf16[256,64]{1,0:T(8,128)(2,1)} %bitcast.7, bf16[256,64]{1,0:T(8,128)(2,1)} %bitcast.8, f32[1,256]{1,0:T(1,128)} %bitcast.13, ...), custom_call_target="tpu_custom_call" | custom-call | tf_op jit(solution)/shard_map/pallas_call | solution.py:1372
  160.7 2.1 %copy.18 = bf16[768,512]{1,0:T(8,128)(2,1)} copy(bf16[768,512]{1,0:T(8,128)(2,1)} %shard_map.154) | data formatting | bytes 1572864
